TPU v7x, 32 devices: a whole 2x2x4 slice. The times are simulated.
32 devices in a mesh: sp: 8 (over z, x), tp: 4 (over y, core).
Axes of the slice: x: 2, y: 2, z: 4, core: 2. Of those that a mesh axis runs over, the one named last changes fastest.
Arguments:
- queries: bfloat16 [2048, 2048], P('sp', 'tp'), may hold values from -6 to 6
- key_matrix: bfloat16 [2048, 2048], P('sp', 'tp'), may hold values from -6 to 6
- value_matrix: bfloat16 [2048, 4096], P('sp', 'tp'), may hold values from -6 to 6
- output_gate_preactivation: bfloat16 [2048, 4096], P('sp', 'tp'), may hold values from -6 to 6
- decay_preactivation: bfloat16 [2048, 2048], P('sp', 'tp')
- extra_log_decay: float32 [2048, 16], P('sp', 'tp'), may hold values from -0.7 to 0
- head_norm_gain: bfloat16 [256], replicated, may hold values from 0.099609375 to 1.8984375
- output_projection: bfloat16 [4096, 2048], P(None, 'tp'), may hold values from -0.09375 to 0.09375
- residual: bfloat16 [2048, 2048], P('sp', 'tp'), may hold values from -210 to 210
- feedforward_gain: bfloat16 [2048], replicated, may hold values from 0.099609375 to 1.8984375
- routing: int32 [2048, 4], P('sp'), may hold values from 0 to 7, all different within a row; in each aligned block of 256 rows (0 to 255, 256 to 511, ...) at most 192 rows name the same one
- router_score: float32 [2048, 4], P('sp'), may hold values from 0.05 to 1
- expert_gate_weight: bfloat16 [2048, 8192], P(None, ('sp', 'tp')), may hold values from -0.125 to 0.125
- expert_up_weight: bfloat16 [2048, 8192], P(None, ('sp', 'tp')), may hold values from -0.125 to 0.125
- expert_down_weight: bfloat16 [8192, 2048], P(('sp', 'tp')), may hold values from -0.1875 to 0.1875
- shared_expert_gate: bfloat16 [2048, 512], P(None, 'tp'), may hold values from -0.125 to 0.125
- shared_expert_up: bfloat16 [2048, 512], P(None, 'tp'), may hold values from -0.125 to 0.125
- shared_expert_down: bfloat16 [512, 2048], P(None, 'tp'), may hold values from -0.25 to 0.25
Outputs:
- layer_out: bfloat16 [2048, 2048], P('sp', 'tp')
Inputs may be any that keep to these rules, and one draw needn't show every extreme that they name: `routing`: each row names 4 different experts. In each aligned block of 256 rows, the rows of one index of sp, no expert is named by more than 192 rows, a bound that some expert reaches in some blocks.
All inputs are finite; a program needn't handle non-finite values.
Results may differ from a plain program's by a relative error of at most 0.01.
Values may be sent and summed in bfloat16 or wider, within the bound.
A program may use at most 128 MiB of HBM per device.

v0:
```python
import jax
import jax.numpy as jnp
from jax import lax
from jax.sharding import PartitionSpec as P

DK = 128
DV = 256
BLOCK_POSITIONS = 64
FF_PARTS = 4
CHUNKS = 4


HIGHEST = lax.Precision.HIGHEST
EPSILON = 1e-06
ROUTE_SCALE = 2.5
GATE_TEMPER = 16.0


def from_partner(value, axis, bit, upward=False):
    mask = 2**bit
    pairs = [(source, source ^ mask) for source in range(lax.axis_size(axis))]
    if upward:
        pairs = [(source, target) for source, target in pairs if source < target]
    return lax.ppermute(value, axis, pairs)


def as_sent(value):
    return jax.tree.map(lambda a: a.astype(jnp.bfloat16) if a.dtype == jnp.float32 else a, value)


def carry_combine(first_part, second_part):
    return (
        first_part[0] * second_part[0],
        second_part[0][..., None] * first_part[1] + second_part[1],
    )


def choose(flag, yes, no):
    return jax.tree.map(lambda a, b: jnp.where(flag, a, b), yes, no)


def prefix(value, axis, join, neutral):
    place = lax.axis_index(axis)
    bits = lax.axis_size(axis).bit_length() - 1
    total, state = value, neutral
    for bit in range(bits):
        upper = (place >> bit) % 2 == 1
        last = bit == bits - 1
        arrived = jax.tree.map(
            lambda a: from_partner(a.astype(jnp.bfloat16), axis, bit, last).astype(a.dtype), total
        )
        state = choose(upper, join(arrived, state), state)
        if not last:
            total = choose(upper, join(arrived, total), join(total, arrived))
    return state


def relative_rows(matrix, place, masks):
    height = matrix.shape[0] // len(masks)
    return jnp.concatenate(
        [lax.dynamic_slice_in_dim(matrix, (place ^ mask) * height, height, 0) for mask in masks], 0
    )


def relative_columns(matrix, place, masks):
    width = matrix.shape[1] // len(masks)
    return jnp.concatenate(
        [lax.dynamic_slice_in_dim(matrix, (place ^ mask) * width, width, 1) for mask in masks], 1
    )


def masks_of(steps, axis):
    masks = [0]
    for step_axis, bit in steps:
        if step_axis == axis:
            masks = masks + [mask ^ (2**bit) for mask in masks]
    return masks


def spread(value, steps):
    for axis, bit in steps:
        arrived = from_partner(value, axis, bit)
        value = jnp.concatenate([value, arrived], 0 if axis == "sp" else 1)
    return value


def collect(value, steps):
    for axis, bit in reversed(steps):
        own, given = jnp.split(value, 2, 0 if axis == "sp" else 1)
        value = (
            own.astype(jnp.float32) + from_partner(given, axis, bit).astype(jnp.float32)
        ).astype(jnp.bfloat16)
    return value


def dot_halves(halves, matrix):
    parts = jnp.split(matrix, 2, 0)
    return sum(
        jnp.dot(half, part, preferred_element_type=jnp.float32)
        for half, part in zip(halves, parts)
    )


def dense_experts(
    mid_local,
    feedforward_gain,
    routing,
    router_score,
    expert_gate_weight,
    expert_up_weight,
    expert_down_weight,
    shared_expert_gate,
    shared_expert_up,
    shared_expert_down,
):
    tokens = mid_local.shape[0]
    hidden_width = expert_gate_weight.shape[1]
    sp_index, tp_index = lax.axis_index("sp"), lax.axis_index("tp")
    sp_steps = [("sp", bit) for bit in range(lax.axis_size("sp").bit_length() - 1)][::-1]
    tp_steps = [("tp", bit) for bit in range(lax.axis_size("tp").bit_length() - 1)][::-1]
    plans = (
        sp_steps + tp_steps,
        sp_steps[:-1] + tp_steps[:-1] + sp_steps[-1:] + tp_steps[-1:],
    )
    column_masks = masks_of(tp_steps, "tp")
    slab = mid_local.shape[1]
    gain = lax.dynamic_slice_in_dim(feedforward_gain, tp_index * slab, slab, 0)
    mid_float = mid_local.astype(jnp.float32)
    scaled = (mid_float * gain.astype(jnp.float32)).astype(jnp.bfloat16)
    squares = jnp.sum(mid_float * mid_float, axis=-1)
    for axis, bit in tp_steps:
        squares = squares + from_partner(squares, axis, bit)
    inverse_own = lax.rsqrt(squares / (slab * lax.axis_size("tp")) + EPSILON)
    inverse_here = spread(inverse_own[None], sp_steps)
    gate = relative_rows(expert_gate_weight, tp_index, column_masks)
    up = relative_rows(expert_up_weight, tp_index, column_masks)
    down = relative_columns(expert_down_weight, tp_index, column_masks)
    shared_gate = relative_rows(shared_expert_gate, tp_index, column_masks)
    shared_up = relative_rows(shared_expert_up, tp_index, column_masks)
    shared_down = relative_rows(shared_expert_down, tp_index, column_masks)
    route_weight = ROUTE_SCALE * router_score / jnp.sum(router_score, axis=1, keepdims=True)
    expert_ids = jnp.arange(lax.axis_size("sp"), dtype=jnp.int32)
    weight_table = jnp.sum(
        jnp.where(routing[:, :, None] == expert_ids, route_weight[:, :, None], 0.0), axis=1
    )
    weight_all = spread(weight_table.T[None], sp_steps)
    weight_here = lax.dynamic_index_in_dim(weight_all, sp_index, 1, False)
    rows = tokens // CHUNKS
    own_halves, routed = [], []
    for chunk in range(CHUNKS):
        steps = plans[chunk % 2]
        axis, bit = steps[-1]
        span = slice(chunk * rows, (chunk + 1) * rows)
        near = spread(scaled[span], steps[:-1])
        halves = (near, from_partner(near, axis, bit))
        own_halves.append([half[:rows] for half in halves])
        row_inverse = inverse_here[:, span].reshape(-1, 1)
        row_weight = weight_here[:, span].reshape(-1, 1)
        hidden = (
            jax.nn.silu(dot_halves(halves, gate) * row_inverse)
            * (dot_halves(halves, up) * row_inverse)
            * row_weight
        ).astype(jnp.bfloat16)
        kept_down, given_down = jnp.split(down, 2, 1)
        given = jnp.dot(hidden, given_down, preferred_element_type=jnp.float32).astype(jnp.bfloat16)
        kept = jnp.dot(hidden, kept_down, preferred_element_type=jnp.float32)
        summed = (kept + from_partner(given, axis, bit).astype(jnp.float32)).astype(jnp.bfloat16)
        routed.append(collect(summed, steps[:-1]))
    own_halves = [jnp.concatenate(parts, 0) for parts in zip(*own_halves)]
    shared_hidden = (
        jax.nn.silu(dot_halves(own_halves, shared_gate) * inverse_own[:, None])
        * (dot_halves(own_halves, shared_up) * inverse_own[:, None])
    ).astype(jnp.bfloat16)
    shared_out = jnp.dot(
        spread(shared_hidden, tp_steps), shared_down, preferred_element_type=jnp.float32
    )
    routed = jnp.concatenate(routed, 0).astype(jnp.float32)
    return (mid_float + routed + shared_out).astype(jnp.bfloat16)


def attention_heads(queries, key_matrix, value_matrix, decay_preactivation, extra_log_decay):
    tokens = queries.shape[0]
    local_head_count = extra_log_decay.shape[1]
    block_count = tokens // BLOCK_POSITIONS
    query_block = queries.astype(jnp.float32).reshape(
        block_count, BLOCK_POSITIONS, local_head_count, DK
    ) * DK ** (-0.5)
    key_block = key_matrix.astype(jnp.float32).reshape(
        block_count, BLOCK_POSITIONS, local_head_count, DK
    )
    value_block = value_matrix.astype(jnp.float32).reshape(
        block_count, BLOCK_POSITIONS, local_head_count, DV
    )
    log_decay_rows = (
        jax.nn.log_sigmoid(decay_preactivation.astype(jnp.float32)).reshape(
            block_count, BLOCK_POSITIONS, local_head_count, DK
        )
        / GATE_TEMPER
    )
    log_decay_rows = (
        log_decay_rows
        + extra_log_decay.reshape(block_count, BLOCK_POSITIONS, local_head_count)[..., None]
    )
    inside = jnp.cumsum(log_decay_rows, axis=1)
    block_total = inside[:, -1]
    query_decay = query_block * jnp.exp(inside)
    key_decay = key_block * jnp.exp(-inside)
    causal = jnp.tril(jnp.ones((BLOCK_POSITIONS, BLOCK_POSITIONS), dtype=bool))
    scores = jnp.where(
        causal, jnp.einsum("nthd,nshd->nhts", query_decay, key_decay, precision=HIGHEST), 0.0
    )
    within = jnp.einsum("nhts,nshv->nthv", scores, value_block, precision=HIGHEST)
    key_end = key_block * jnp.exp(block_total[:, None] - inside)
    update = jnp.einsum("nshd,nshv->nhdv", key_end, value_block, precision=HIGHEST)
    before = jnp.cumsum(block_total, axis=0) - block_total
    ending = jnp.concatenate([before, (before[-1] + block_total[-1])[None]], axis=0)
    after_block = before + block_total
    earlier_mask = jnp.arange(block_count + 1)[:, None] > jnp.arange(block_count)[None, :]
    span_logs = jnp.where(
        earlier_mask[:, :, None, None], ending[:, None] - after_block[None], -1e30
    )
    states = jnp.einsum("nmhd,mhdv->nhdv", jnp.exp(span_logs), update, precision=HIGHEST)
    passed = jnp.einsum("nthd,nhdv->nthv", query_decay, states[:block_count], precision=HIGHEST)
    query_start = query_block * jnp.exp(inside + before[:, None])
    return (within + passed, query_start, jnp.exp(ending[block_count]), states[block_count])


def body(
    queries,
    key_matrix,
    value_matrix,
    output_gate_preactivation,
    decay_preactivation,
    extra_log_decay,
    head_norm_gain,
    output_projection,
    residual,
    feedforward_gain,
    routing,
    router_score,
    expert_gate_weight,
    expert_up_weight,
    expert_down_weight,
    shared_expert_gate,
    shared_expert_up,
    shared_expert_down,
):
    tokens = queries.shape[0]
    local_head_count = extra_log_decay.shape[1]
    local_part, query_start, dev_decay, dev_update = attention_heads(
        queries, key_matrix, value_matrix, decay_preactivation, extra_log_decay
    )
    _, entering = prefix(
        (dev_decay, dev_update),
        "sp",
        carry_combine,
        (jnp.ones_like(dev_decay), jnp.zeros_like(dev_update)),
    )
    attention_output = local_part + jnp.einsum(
        "nthd,hdv->nthv", query_start, entering, precision=HIGHEST
    )
    attention_output = attention_output.reshape(tokens, local_head_count, DV)
    inverse_rms = lax.rsqrt(
        jnp.mean(attention_output * attention_output, axis=-1, keepdims=True) + EPSILON
    )
    gate_act = jax.nn.silu(
        output_gate_preactivation.astype(jnp.float32).reshape(tokens, local_head_count, DV)
    )
    head_rows = (
        (attention_output * inverse_rms * head_norm_gain.astype(jnp.float32) * gate_act)
        .reshape(tokens, local_head_count * DV)
        .astype(jnp.bfloat16)
    )
    tp_steps = [("tp", bit) for bit in range(lax.axis_size("tp").bit_length() - 1)][::-1]
    projected = jnp.dot(
        spread(head_rows, tp_steps),
        relative_rows(output_projection, lax.axis_index("tp"), masks_of(tp_steps, "tp")),
        preferred_element_type=jnp.float32,
    )
    mid_local = (residual.astype(jnp.float32) + projected).astype(jnp.bfloat16)
    most = 3 * tokens * routing.shape[1] // (2 * lax.axis_size("sp"))
    if lax.axis_size("tp") == FF_PARTS and 2 * most >= tokens:
        return dense_experts(
            mid_local,
            feedforward_gain,
            routing,
            router_score,
            expert_gate_weight,
            expert_up_weight,
            expert_down_weight,
            shared_expert_gate,
            shared_expert_up,
            shared_expert_down,
        )
    mid_rows = lax.all_gather(mid_local, "tp", axis=1, tiled=True).astype(jnp.float32)
    normed = (
        mid_rows
        * lax.rsqrt(jnp.mean(mid_rows * mid_rows, axis=-1, keepdims=True) + EPSILON)
        * feedforward_gain.astype(jnp.float32)
    ).astype(jnp.bfloat16)
    shared_pre = jnp.dot(normed, shared_expert_gate, preferred_element_type=jnp.float32)
    shared_lin = jnp.dot(normed, shared_expert_up, preferred_element_type=jnp.float32)
    shared_hidden = (jax.nn.silu(shared_pre) * shared_lin).astype(jnp.bfloat16)
    senders = lax.axis_size("sp")
    tp_count = lax.axis_size("tp")
    tp_bits = tp_count.bit_length() - 1
    tp_index = lax.axis_index("tp")
    groups = tp_count // FF_PARTS
    group_here = tp_index // FF_PARTS
    part_here = tp_index % FF_PARTS
    model_width = normed.shape[1]
    picks = routing.shape[1]
    expert_total = senders * groups
    rows_most = max(2, 3 * tokens * picks // (2 * expert_total))
    slot_count = senders * rows_most
    flat_expert = routing.reshape(-1)
    one_hot = (flat_expert[:, None] == jnp.arange(expert_total, dtype=jnp.int32)[None, :]).astype(
        jnp.int32
    )
    rank_before = jnp.sum((jnp.cumsum(one_hot, axis=0) - one_hot) * one_hot, axis=1)
    owned = flat_expert % groups == group_here
    slot_index = jnp.where(owned, flat_expert // groups * rows_most + rank_before, slot_count)
    token_index = jnp.arange(flat_expert.shape[0], dtype=jnp.int32) // picks
    part_width = model_width // FF_PARTS
    normed_part = lax.dynamic_slice_in_dim(normed, part_here * part_width, part_width, 1)
    outgoing = (
        jnp.zeros((slot_count, part_width), jnp.bfloat16)
        .at[slot_index]
        .set(normed_part[token_index], mode="drop")
    )
    arrived = lax.all_to_all(
        outgoing.reshape(senders, rows_most, part_width),
        "sp",
        split_axis=0,
        concat_axis=0,
        tiled=True,
    )
    for bit in range(2):
        partner_cols = from_partner(arrived, "tp", bit)
        upper = (tp_index >> bit) % 2
        arrived = jnp.where(
            upper == 1,
            jnp.concatenate([partner_cols, arrived], axis=2),
            jnp.concatenate([arrived, partner_cols], axis=2),
        )
    rows_in = arrived.reshape(slot_count, model_width)
    gate_pre = jnp.dot(rows_in, expert_gate_weight, preferred_element_type=jnp.float32)
    up_pre = jnp.dot(rows_in, expert_up_weight, preferred_element_type=jnp.float32)
    routed_hidden = (jax.nn.silu(gate_pre) * up_pre).astype(jnp.bfloat16)
    partial_out = jnp.dot(routed_hidden, expert_down_weight, preferred_element_type=jnp.float32)
    slab_width = model_width // tp_count
    partial_out = partial_out.reshape(slot_count, groups, FF_PARTS, slab_width)
    for bit in (1, 0):
        paired = partial_out.reshape(slot_count, groups, 2, 2**bit, slab_width)
        upper = (tp_index >> bit) % 2
        kept = lax.dynamic_index_in_dim(paired, upper, 2, keepdims=False)
        given = lax.dynamic_index_in_dim(paired, 1 - upper, 2, keepdims=False)
        partial_out = kept + from_partner(given.astype(jnp.bfloat16), "tp", bit).astype(given.dtype)
    expert_out = partial_out.reshape(senders, rows_most, groups, slab_width).astype(jnp.bfloat16)
    shared_out = jnp.dot(
        lax.all_gather(shared_hidden, "tp", axis=1, tiled=True),
        shared_expert_down,
        preferred_element_type=jnp.float32,
    )
    returned = lax.all_to_all(expert_out, "sp", split_axis=0, concat_axis=0, tiled=True).reshape(
        slot_count, groups, slab_width
    )
    safe_slot = jnp.minimum(slot_index, slot_count - 1)
    route_weight = ROUTE_SCALE * router_score / jnp.sum(router_score, axis=1, keepdims=True)
    pair_weight = jnp.where(owned, route_weight.reshape(-1), 0.0)
    picked = returned[safe_slot].astype(jnp.float32) * pair_weight[:, None, None]
    routed_part = jnp.sum(picked.reshape(tokens, picks, groups, slab_width), axis=1)
    for bit in range(tp_bits - 1, 1, -1):
        paired = routed_part.reshape(tokens, 2, 2 ** (bit - 2), slab_width)
        upper = (tp_index >> bit) % 2
        kept = lax.dynamic_index_in_dim(paired, upper, 1, keepdims=False)
        given = lax.dynamic_index_in_dim(paired, 1 - upper, 1, keepdims=False)
        routed_part = kept + from_partner(as_sent(given), "tp", bit).astype(given.dtype)
    routed = routed_part.reshape(tokens, slab_width)
    return (mid_local.astype(jnp.float32) + routed + shared_out).astype(jnp.bfloat16)


def solution(mesh):
    return jax.shard_map(
        body,
        mesh=mesh,
        in_specs=(
            P("sp", "tp"),
            P("sp", "tp"),
            P("sp", "tp"),
            P("sp", "tp"),
            P("sp", "tp"),
            P("sp", "tp"),
            P(),
            P(None, "tp"),
            P("sp", "tp"),
            P(),
            P("sp", None),
            P("sp", None),
            P(None, ("sp", "tp")),
            P(None, ("sp", "tp")),
            P(("sp", "tp"), None),
            P(None, "tp"),
            P(None, "tp"),
            P(None, "tp"),
        ),
        out_specs=P("sp", "tp"),
        check_vma=False,
    )
```

profile of v0, /device:TPU:0, one launch (start us, length us, event | category | flops | bytes accessed | tf_op | source)
XLA Modules:
  0.0 249.1 jit_solution(12266261581365429488)
XLA Ops:
  4.0 1.3 exponential_multiply_fusion
  6.4 6.1 %convolution_bitcast_fusion = f32[5,4,128,256]{3,0,2,1:T(8,128)S(1)} fusion(f32[4,4,128,256]{3,2,1,0:T(8,128)S(1)} %fusion.63, f32[4,4,128]{0,2,1:T(8,128)S(1)} %copy.84, f32[5,4,128]{0,2,1:T(8,128)S(1)} %copy.83, pred[5,4]{0,1:T(4,128)(4,1)S(1)} %iota_compare_fusion.2), kind=kOutput, calls=%fused_computation.8 | convolution fusion | flops 31477760 | bytes 4737044 | tf_op jit(solution)/shard_map/nmhd,mhdv->nhdv/dot_general | solution.py:222
  13.8 3.0 %collective-permute-start.2 = (bf16[4,128,256]{2,1,0:T(8,128)(2,1)}, bf16[4,128,256]{2,1,0:T(8,128)(2,1)S(1)}, u32[]{:S(2)}, u32[]{:S(2)}) collective-permute-start(bf16[4,128,256]{2,1,0:T(8,128)(2,1)} %bitcast.89), channel_id=1, source_target_pairs={{0,4},{4,0},{8,12},{12,8},{16,20},{20,16},{24,28},{28,24},{1,5},{5... | collective-permute-start | bytes 786440 | tf_op jit(solution)/shard_map/ppermute | solution.py:24
  17.2 11.9 %fusion.16 = f32[4,64,4,256]{3,1,2,0:T(8,128)S(1)} fusion(f32[4,4,128,256]{3,0,2,1:T(4,128)S(1)} %slice.115, f32[4,64,4,128]{3,2,1,0:T(4,128)S(1)} %get-tuple-element.28), kind=kOutput, calls=%fused_computation.26 | convolution fusion | flops 402653184 | bytes 3670016 | tf_op jit(solution)/shard_map/nthd,nhdv->nthv/dot_general | solution.py:223
  29.2 1.8 convolution_select_fusion
  31.0 2.0 collective-permute-start.1
  34.0 1.6 fusion.20
  35.6 5.8 %collective-permute-done.3 = bf16[4,128,256]{2,1,0:T(8,128)(2,1)} collective-permute-done((bf16[4,128,256]{2,1,0:T(8,128)(2,1)}, bf16[4,128,256]{2,1,0:T(8,128)(2,1)}, u32[]{:S(2)}, u32[]{:S(2)}) %collective-permute-start.3) | collective-permute-done | bytes 262176 | tf_op jit(solution)/shard_map/ppermute | solution.py:24
  42.8 4.5 %collective-permute-start.4 = (bf16[4,128,256]{2,1,0:T(8,128)(2,1)S(1)}, bf16[4,128,256]{2,1,0:T(8,128)(2,1)S(1)}, u32[]{:S(2)}, u32[]{:S(2)}) collective-permute-start(bf16[4,128,256]{2,1,0:T(8,128)(2,1)S(1)} %fusion.43), channel_id=1, source_target_pairs={{0,16},{4,20},{8,24},{12,28},{1,17},{5,21},{9,25},{13,29},{2,18},{... | collective-permute-start | bytes 786440 | tf_op jit(solution)/shard_map/ppermute | solution.py:24
  47.3 3.8 %collective-permute-done.4 = bf16[4,128,256]{2,1,0:T(8,128)(2,1)S(1)} collective-permute-done((bf16[4,128,256]{2,1,0:T(8,128)(2,1)S(1)}, bf16[4,128,256]{2,1,0:T(8,128)(2,1)S(1)}, u32[]{:S(2)}, u32[]{:S(2)}) %collective-permute-start.4) | collective-permute-done | bytes 262176 | tf_op jit(solution)/shard_map/ppermute | solution.py:24
  51.2 2.4 multiply_reduce_fusion
  55.7 1.6 collective-permute-start.5
  57.3 9.6 %collective-permute-done.5 = bf16[256,1024]{1,0:T(8,128)(2,1)S(1)} collective-permute-done((bf16[256,1024]{1,0:T(8,128)(2,1)S(1)}, bf16[256,1024]{1,0:T(8,128)(2,1)S(1)}, u32[]{:S(2)}, u32[]{:S(2)}) %collective-permute-start.5) | collective-permute-done | bytes 524320 | tf_op jit(solution)/shard_map/ppermute | solution.py:24
  68.1 3.5 %collective-permute-start.17 = (f32[1,8,256]{2,1,0:T(8,128)S(1)}, f32[1,8,256]{2,1,0:T(8,128)S(1)}, u32[]{:S(2)}, u32[]{:S(2)}) collective-permute-start(f32[1,8,256]{2,1,0:T(8,128)S(1)} %bitcast.97), channel_id=1, source_target_pairs={{0,16},{4,20},{8,24},{12,28},{16,0},{20,4},{24,8},{28,12},{1,17},{... | collective-permute-start | bytes 24584 | tf_op jit(solution)/shard_map/ppermute | solution.py:24
  71.7 2.2 constant_dynamic-slice_fusion.5
  74.0 1.5 constant_dynamic-slice_fusion.19
  75.4 1.5 copy-done
  76.9 1.7 constant_dynamic-slice_fusion.27
  79.4 7.7 %collective-permute-start.18 = (f32[2,8,256]{2,1,0:T(8,128)S(1)}, f32[2,8,256]{2,1,0:T(8,128)S(1)}, u32[]{:S(2)}, u32[]{:S(2)}) collective-permute-start(f32[2,8,256]{2,1,0:T(8,128)S(1)} %pad_maximum_fusion.33), channel_id=1, source_target_pairs={{0,8},{4,12},{8,0},{12,4},{16,24},{20,28},{24,16},{28,20},{1,9},{5... | collective-permute-start | bytes 49160 | tf_op jit(solution)/shard_map/ppermute | solution.py:24
  87.1 4.2 %fusion.47 = (f32[256]{0:T(256)S(1)}, bf16[256,512]{1,0:T(8,128)(2,1)S(1)}, bf16[256,512]{1,0:T(8,128)(2,1)}) fusion(f32[512]{0:T(512)S(1)} %dynamic-slice_convert_fusion, bf16[1024,512]{1,0:T(8,128)(2,1)} %get-tuple-element.13, bf16[1024,512]{1,0:T(8,128)(2,1)} %get-tuple-element.14, bf16[1024,512]{1,0:T(8,128)(2,1)} %get-tuple-element.12, ...), kind=kOutput, calls=%fused_computation.90 | convolution fusion | flops 1097858816 | bytes 7080960 | tf_op jit(solution)/shard_map/dot_general | solution.py:275
  91.5 1.5 collective-permute-start.12
  93.0 1.5 collective-permute-start.19
  94.5 2.8 %collective-permute-start.25 = (bf16[64,512]{1,0:T(8,128)(2,1)S(1)}, bf16[64,512]{1,0:T(8,128)(2,1)S(1)}, u32[]{:S(2)}, u32[]{:S(2)}) collective-permute-start(bf16[64,512]{1,0:T(8,128)(2,1)S(1)} %get-tuple-element.48), channel_id=1, source_target_pairs={{0,16},{4,20},{8,24},{12,28},{16,0},{20,4},{24,8},{28,12},{1,17},{... | collective-permute-start | bytes 196616 | tf_op jit(solution)/shard_map/ppermute | solution.py:24
  97.4 2.8 %collective-permute-start.45 = (bf16[64,512]{1,0:T(8,128)(2,1)S(1)}, bf16[64,512]{1,0:T(8,128)(2,1)S(1)}, u32[]{:S(2)}, u32[]{:S(2)}) collective-permute-start(bf16[64,512]{1,0:T(8,128)(2,1)S(1)} %get-tuple-element.46), channel_id=1, source_target_pairs={{0,16},{4,20},{8,24},{12,28},{16,0},{20,4},{24,8},{28,12},{1,17},{... | collective-permute-start | bytes 196616 | tf_op jit(solution)/shard_map/ppermute | solution.py:24
  100.4 3.1 %collective-permute-done.25 = bf16[64,512]{1,0:T(8,128)(2,1)S(1)} collective-permute-done((bf16[64,512]{1,0:T(8,128)(2,1)S(1)}, bf16[64,512]{1,0:T(8,128)(2,1)S(1)}, u32[]{:S(2)}, u32[]{:S(2)}) %collective-permute-start.25) | collective-permute-done | bytes 65568 | tf_op jit(solution)/shard_map/ppermute | solution.py:24
  103.5 1.5 collective-permute-done.35
  107.1 2.7 %collective-permute-done.8 = bf16[128,512]{1,0:T(8,128)(2,1)S(1)} collective-permute-done((bf16[128,512]{1,0:T(8,128)(2,1)S(1)}, bf16[128,512]{1,0:T(8,128)(2,1)S(1)}, u32[]{:S(2)}, u32[]{:S(2)}) %collective-permute-start.8) | collective-permute-done | bytes 131104 | tf_op jit(solution)/shard_map/ppermute | solution.py:24
  109.8 2.8 %collective-permute-done.26 = bf16[128,512]{1,0:T(8,128)(2,1)S(1)} collective-permute-done((bf16[128,512]{1,0:T(8,128)(2,1)S(1)}, bf16[128,512]{1,0:T(8,128)(2,1)S(1)}, u32[]{:S(2)}, u32[]{:S(2)}) %collective-permute-start.26) | collective-permute-done | bytes 131104 | tf_op jit(solution)/shard_map/ppermute | solution.py:24
  113.8 1.7 collective-permute-done.36
  117.0 1.5 collective-permute-start.37
  120.5 2.9 %collective-permute-done.27 = bf16[256,512]{1,0:T(8,128)(2,1)S(1)} collective-permute-done((bf16[256,512]{1,0:T(8,128)(2,1)S(1)}, bf16[256,512]{1,0:T(8,128)(2,1)S(1)}, u32[]{:S(2)}, u32[]{:S(2)}) %collective-permute-start.27) | collective-permute-done | bytes 262176 | tf_op jit(solution)/shard_map/ppermute | solution.py:24
  124.8 2.5 %collective-permute-start.28 = (bf16[256,1024]{1,0:T(8,128)(2,1)S(1)}, bf16[256,1024]{1,0:T(8,128)(2,1)S(1)}, u32[]{:S(2)}, u32[]{:S(2)}) collective-permute-start(bf16[256,1024]{1,0:T(8,128)(2,1)S(1)} %pad_maximum_fusion.12), channel_id=1, source_target_pairs={{0,4},{4,0},{8,12},{12,8},{16,20},{20,16},{24,28},{28,24},{1,5},{5... | collective-permute-start | bytes 1572872 | tf_op jit(solution)/shard_map/ppermute | solution.py:24
  127.3 1.7 collective-permute-done.47
  130.4 2.5 %collective-permute-start.48 = (bf16[256,1024]{1,0:T(8,128)(2,1)S(1)}, bf16[256,1024]{1,0:T(8,128)(2,1)S(1)}, u32[]{:S(2)}, u32[]{:S(2)}) collective-permute-start(bf16[256,1024]{1,0:T(8,128)(2,1)S(1)} %pad_maximum_fusion.14), channel_id=1, source_target_pairs={{0,4},{4,0},{8,12},{12,8},{16,20},{20,16},{24,28},{28,24},{1,5},{5... | collective-permute-start | bytes 1572872 | tf_op jit(solution)/shard_map/ppermute | solution.py:24
  132.9 7.3 %collective-permute-done.10 = bf16[512,512]{1,0:T(8,128)(2,1)S(1)} collective-permute-done((bf16[512,512]{1,0:T(8,128)(2,1)S(1)}, bf16[512,512]{1,0:T(8,128)(2,1)S(1)}, u32[]{:S(2)}, u32[]{:S(2)}) %collective-permute-start.10) | collective-permute-done | bytes 524320 | tf_op jit(solution)/shard_map/ppermute | solution.py:24
  140.3 2.4 collective-permute-start.14
  144.0 5.9 %collective-permute-done.38 = bf16[512,512]{1,0:T(8,128)(2,1)S(1)} collective-permute-done((bf16[512,512]{1,0:T(8,128)(2,1)S(1)}, bf16[512,512]{1,0:T(8,128)(2,1)S(1)}, u32[]{:S(2)}, u32[]{:S(2)}) %collective-permute-start.38) | collective-permute-done | bytes 524320 | tf_op jit(solution)/shard_map/ppermute | solution.py:24
  152.0 3.5 %collective-permute-done.15 = f32[2,256]{1,0:T(2,128)S(1)} collective-permute-done((f32[2,256]{1,0:T(2,128)S(1)}, f32[2,256]{1,0:T(2,128)S(1)}, u32[]{:S(2)}, u32[]{:S(2)}) %collective-permute-start.15) | collective-permute-done | bytes 2080 | tf_op jit(solution)/shard_map/ppermute | solution.py:24
  156.1 1.4 collective-permute-start.16
  169.8 1.6 collective-permute-start.55
  171.5 1.8 fusion.134
  173.3 1.7 fusion.138
  177.1 1.8 fusion.133
  178.9 1.8 fusion.137
  182.8 1.7 fusion.132
  184.5 1.7 fusion.136
  188.0 1.7 fusion.135
  190.2 1.7 fusion.131
  195.4 1.4 collective-permute-start.31
  197.3 1.5 collective-permute-start.41
  200.1 9.1 %collective-permute-done.21 = bf16[512,512]{1,0:T(8,128)(2,1)S(1)} collective-permute-done((bf16[512,512]{1,0:T(8,128)(2,1)S(1)}, bf16[512,512]{1,0:T(8,128)(2,1)S(1)}, u32[]{:S(2)}, u32[]{:S(2)}) %collective-permute-start.21) | collective-permute-done | bytes 524320 | tf_op jit(solution)/shard_map/ppermute | solution.py:24
  209.4 1.4 collective-permute-start.22
  212.1 8.4 %collective-permute-done.41 = bf16[512,512]{1,0:T(8,128)(2,1)S(1)} collective-permute-done((bf16[512,512]{1,0:T(8,128)(2,1)S(1)}, bf16[512,512]{1,0:T(8,128)(2,1)S(1)}, u32[]{:S(2)}, u32[]{:S(2)}) %collective-permute-start.41) | collective-permute-done | bytes 524320 | tf_op jit(solution)/shard_map/ppermute | solution.py:24
  220.6 1.4 collective-permute-start.42
  223.3 3.9 %collective-permute-done.22 = bf16[256,512]{1,0:T(8,128)(2,1)S(1)} collective-permute-done((bf16[256,512]{1,0:T(8,128)(2,1)S(1)}, bf16[256,512]{1,0:T(8,128)(2,1)S(1)}, u32[]{:S(2)}, u32[]{:S(2)}) %collective-permute-start.22) | collective-permute-done | bytes 262176 | tf_op jit(solution)/shard_map/ppermute | solution.py:24
  227.6 1.9 collective-permute-start.33
  229.5 2.2 collective-permute-done.42
  232.2 1.9 collective-permute-start.53
  234.3 3.0 %collective-permute-start.34 = (bf16[64,512]{1,0:T(8,128)(2,1)S(1)}, bf16[64,512]{1,0:T(8,128)(2,1)S(1)}, u32[]{:S(2)}, u32[]{:S(2)}) collective-permute-start(bf16[64,512]{1,0:T(8,128)(2,1)S(1)} %split.171), channel_id=1, source_target_pairs={{0,16},{4,20},{8,24},{12,28},{16,0},{20,4},{24,8},{28,12},{1,17},{... | collective-permute-start | bytes 196616 | tf_op jit(solution)/shard_map/ppermute | solution.py:24
  237.3 2.6 %collective-permute-done.43 = bf16[128,512]{1,0:T(8,128)(2,1)S(1)} collective-permute-done((bf16[128,512]{1,0:T(8,128)(2,1)S(1)}, bf16[128,512]{1,0:T(8,128)(2,1)S(1)}, u32[]{:S(2)}, u32[]{:S(2)}) %collective-permute-start.43) | collective-permute-done | bytes 131104 | tf_op jit(solution)/shard_map/ppermute | solution.py:24
  240.0 1.5 collective-permute-done.53
  241.6 1.5 collective-permute-start.54
  243.3 2.1 collective-permute-done.34
  245.4 1.5 collective-permute-done.44
  (355 shorter events, 56.5 us)
Async XLA Ops:
  13.8 19.2 %collective-permute-start.2 = (bf16[4,128,256]{2,1,0:T(8,128)(2,1)}, bf16[4,128,256]{2,1,0:T(8,128)(2,1)S(1)}, u32[]{:S(2)}, u32[]{:S(2)}) collective-permute-start(bf16[4,128,256]{2,1,0:T(8,128)(2,1)} %bitcast.89), channel_id=1, source_target_pairs={{0,4},{4,0},{8,12},{12,8},{16,20},{20,16},{24,28},{28,24},{1,5},{5... | collective-permute-start | bytes 786440 | tf_op jit(solution)/shard_map/ppermute | solution.py:24
  16.8 14.2 %collective-permute-start = (bf16[4,128]{1,0:T(4,128)(2,1)S(1)}, bf16[4,128]{1,0:T(4,128)(2,1)S(1)}, u32[]{:S(2)}, u32[]{:S(2)}) collective-permute-start(bf16[4,128]{1,0:T(4,128)(2,1)S(1)} %get-tuple-element.7), channel_id=1, source_target_pairs={{0,4},{4,0},{8,12},{12,8},{16,20},{20,16},{24,28},{28,24},{1,5},{5... | collective-permute-start | bytes 3080 | tf_op jit(solution)/shard_map/ppermute | solution.py:24
  31.0 4.6 %collective-permute-start.1 = (bf16[4,128]{1,0:T(4,128)(2,1)S(1)}, bf16[4,128]{1,0:T(4,128)(2,1)S(1)}, u32[]{:S(2)}, u32[]{:S(2)}) collective-permute-start(bf16[4,128]{1,0:T(4,128)(2,1)S(1)} %get-tuple-element.5), channel_id=1, source_target_pairs={{0,8},{4,12},{8,0},{12,4},{16,24},{20,28},{24,16},{28,20},{1,9},{5... | collective-permute-start | bytes 3080 | tf_op jit(solution)/shard_map/ppermute | solution.py:24
  33.9 7.5 %collective-permute-start.3 = (bf16[4,128,256]{2,1,0:T(8,128)(2,1)}, bf16[4,128,256]{2,1,0:T(8,128)(2,1)}, u32[]{:S(2)}, u32[]{:S(2)}) collective-permute-start(bf16[4,128,256]{2,1,0:T(8,128)(2,1)} %fusion.104), channel_id=1, source_target_pairs={{0,8},{4,12},{8,0},{12,4},{16,24},{20,28},{24,16},{28,20},{1,9},{5... | collective-permute-start | bytes 786440 | tf_op jit(solution)/shard_map/ppermute | solution.py:24
  42.8 8.4 %collective-permute-start.4 = (bf16[4,128,256]{2,1,0:T(8,128)(2,1)S(1)}, bf16[4,128,256]{2,1,0:T(8,128)(2,1)S(1)}, u32[]{:S(2)}, u32[]{:S(2)}) collective-permute-start(bf16[4,128,256]{2,1,0:T(8,128)(2,1)S(1)} %fusion.43), channel_id=1, source_target_pairs={{0,16},{4,20},{8,24},{12,28},{1,17},{5,21},{9,25},{13,29},{2,18},{... | collective-permute-start | bytes 786440 | tf_op jit(solution)/shard_map/ppermute | solution.py:24
  55.7 11.2 %collective-permute-start.5 = (bf16[256,1024]{1,0:T(8,128)(2,1)S(1)}, bf16[256,1024]{1,0:T(8,128)(2,1)S(1)}, u32[]{:S(2)}, u32[]{:S(2)}) collective-permute-start(bf16[256,1024]{1,0:T(8,128)(2,1)S(1)} %fusion.38), channel_id=1, source_target_pairs={{0,2},{1,3},{2,0},{3,1},{4,6},{5,7},{6,4},{7,5},{8,10},{9,11},{10,... | collective-permute-start | bytes 1572872 | tf_op jit(solution)/shard_map/ppermute | solution.py:24
  68.1 19.1 %collective-permute-start.6 = (bf16[256,2048]{1,0:T(8,128)(2,1)}, bf16[256,2048]{1,0:T(8,128)(2,1)}, u32[]{:S(2)}, u32[]{:S(2)}) collective-permute-start(bf16[256,2048]{1,0:T(8,128)(2,1)} %pad_maximum_fusion), channel_id=1, source_target_pairs={{0,1},{1,0},{2,3},{3,2},{4,5},{5,4},{6,7},{7,6},{8,9},{9,8},{10,11... | collective-permute-start | bytes 3145736 | tf_op jit(solution)/shard_map/ppermute | solution.py:24
  68.1 11.3 %collective-permute-start.17 = (f32[1,8,256]{2,1,0:T(8,128)S(1)}, f32[1,8,256]{2,1,0:T(8,128)S(1)}, u32[]{:S(2)}, u32[]{:S(2)}) collective-permute-start(f32[1,8,256]{2,1,0:T(8,128)S(1)} %bitcast.97), channel_id=1, source_target_pairs={{0,16},{4,20},{8,24},{12,28},{16,0},{20,4},{24,8},{28,12},{1,17},{... | collective-permute-start | bytes 24584 | tf_op jit(solution)/shard_map/ppermute | solution.py:24
  79.4 13.6 %collective-permute-start.18 = (f32[2,8,256]{2,1,0:T(8,128)S(1)}, f32[2,8,256]{2,1,0:T(8,128)S(1)}, u32[]{:S(2)}, u32[]{:S(2)}) collective-permute-start(f32[2,8,256]{2,1,0:T(8,128)S(1)} %pad_maximum_fusion.33), channel_id=1, source_target_pairs={{0,8},{4,12},{8,0},{12,4},{16,24},{20,28},{24,16},{28,20},{1,9},{5... | collective-permute-start | bytes 49160 | tf_op jit(solution)/shard_map/ppermute | solution.py:24
  91.3 8.9 %collective-permute-start.7 = (bf16[64,512]{1,0:T(8,128)(2,1)S(1)}, bf16[64,512]{1,0:T(8,128)(2,1)S(1)}, u32[]{:S(2)}, u32[]{:S(2)}) collective-permute-start(bf16[64,512]{1,0:T(8,128)(2,1)S(1)} %get-tuple-element.45), channel_id=1, source_target_pairs={{0,16},{4,20},{8,24},{12,28},{16,0},{20,4},{24,8},{28,12},{1,17},{... | collective-permute-start | bytes 196616 | tf_op jit(solution)/shard_map/ppermute | solution.py:24
  91.5 5.9 %collective-permute-start.12 = (f32[256]{0:T(256)S(1)}, f32[256]{0:T(256)S(1)}, u32[]{:S(2)}, u32[]{:S(2)}) collective-permute-start(f32[256]{0:T(256)S(1)} %get-tuple-element.49), channel_id=1, source_target_pairs={{0,2},{1,3},{2,0},{3,1},{4,6},{5,7},{6,4},{7,5},{8,10},{9,11},{10,... | collective-permute-start | bytes 3080 | tf_op jit(solution)/shard_map/ppermute | solution.py:24
  93.0 58.9 %collective-permute-start.19 = (f32[4,8,256]{2,1,0:T(8,128)S(1)}, f32[4,8,256]{2,1,0:T(8,128)S(1)}, u32[]{:S(2)}, u32[]{:S(2)}) collective-permute-start(f32[4,8,256]{2,1,0:T(8,128)S(1)} %pad_maximum_fusion.32), channel_id=1, source_target_pairs={{0,4},{4,0},{8,12},{12,8},{16,20},{20,16},{24,28},{28,24},{1,5},{5... | collective-permute-start | bytes 98312 | tf_op jit(solution)/shard_map/ppermute | solution.py:24
  94.5 8.9 %collective-permute-start.25 = (bf16[64,512]{1,0:T(8,128)(2,1)S(1)}, bf16[64,512]{1,0:T(8,128)(2,1)S(1)}, u32[]{:S(2)}, u32[]{:S(2)}) collective-permute-start(bf16[64,512]{1,0:T(8,128)(2,1)S(1)} %get-tuple-element.48), channel_id=1, source_target_pairs={{0,16},{4,20},{8,24},{12,28},{16,0},{20,4},{24,8},{28,12},{1,17},{... | collective-permute-start | bytes 196616 | tf_op jit(solution)/shard_map/ppermute | solution.py:24
  97.3 7.6 %collective-permute-start.35 = (bf16[64,512]{1,0:T(8,128)(2,1)S(1)}, bf16[64,512]{1,0:T(8,128)(2,1)S(1)}, u32[]{:S(2)}, u32[]{:S(2)}) collective-permute-start(bf16[64,512]{1,0:T(8,128)(2,1)S(1)} %get-tuple-element.47), channel_id=1, source_target_pairs={{0,16},{4,20},{8,24},{12,28},{16,0},{20,4},{24,8},{28,12},{1,17},{... | collective-permute-start | bytes 196616 | tf_op jit(solution)/shard_map/ppermute | solution.py:24
  97.4 8.5 %collective-permute-start.45 = (bf16[64,512]{1,0:T(8,128)(2,1)S(1)}, bf16[64,512]{1,0:T(8,128)(2,1)S(1)}, u32[]{:S(2)}, u32[]{:S(2)}) collective-permute-start(bf16[64,512]{1,0:T(8,128)(2,1)S(1)} %get-tuple-element.46), channel_id=1, source_target_pairs={{0,16},{4,20},{8,24},{12,28},{16,0},{20,4},{24,8},{28,12},{1,17},{... | collective-permute-start | bytes 196616 | tf_op jit(solution)/shard_map/ppermute | solution.py:24
  100.3 42.4 %copy-start.14 = (bf16[64,512]{1,0:T(8,128)(2,1)}, bf16[64,512]{1,0:T(8,128)(2,1)S(1)}, u32[]{:S(2)}) copy-start(bf16[64,512]{1,0:T(8,128)(2,1)S(1)} %collective-permute-done.7) | copy-start | bytes 196612
  100.3 30.1 %collective-permute-start.13 = (f32[256]{0:T(256)S(1)}, f32[256]{0:T(256)S(1)}, u32[]{:S(2)}, u32[]{:S(2)}) collective-permute-start(f32[256]{0:T(256)S(1)} %add.312), channel_id=1, source_target_pairs={{0,1},{1,0},{2,3},{3,2},{4,5},{5,4},{6,7},{7,6},{8,9},{9,8},{10,11... | collective-permute-start | bytes 3080 | tf_op jit(solution)/shard_map/ppermute | solution.py:24
  103.4 39.5 %copy-start.12 = (bf16[64,512]{1,0:T(8,128)(2,1)}, bf16[64,512]{1,0:T(8,128)(2,1)S(1)}, u32[]{:S(2)}) copy-start(bf16[64,512]{1,0:T(8,128)(2,1)S(1)} %collective-permute-done.25) | copy-start | bytes 196612
  103.4 6.4 %collective-permute-start.8 = (bf16[128,512]{1,0:T(8,128)(2,1)S(1)}, bf16[128,512]{1,0:T(8,128)(2,1)S(1)}, u32[]{:S(2)}, u32[]{:S(2)}) collective-permute-start(bf16[128,512]{1,0:T(8,128)(2,1)S(1)} %pad_maximum_fusion.21), channel_id=1, source_target_pairs={{0,8},{4,12},{8,0},{12,4},{16,24},{20,28},{24,16},{28,20},{1,9},{5... | collective-permute-start | bytes 393224 | tf_op jit(solution)/shard_map/ppermute | solution.py:24
  104.9 45.0 %copy-start.10 = (bf16[64,512]{1,0:T(8,128)(2,1)}, bf16[64,512]{1,0:T(8,128)(2,1)S(1)}, u32[]{:S(2)}) copy-start(bf16[64,512]{1,0:T(8,128)(2,1)S(1)} %collective-permute-done.35) | copy-start | bytes 196612
  104.9 7.7 %collective-permute-start.26 = (bf16[128,512]{1,0:T(8,128)(2,1)S(1)}, bf16[128,512]{1,0:T(8,128)(2,1)S(1)}, u32[]{:S(2)}, u32[]{:S(2)}) collective-permute-start(bf16[128,512]{1,0:T(8,128)(2,1)S(1)} %pad_maximum_fusion.22), channel_id=1, source_target_pairs={{0,8},{4,12},{8,0},{12,4},{16,24},{20,28},{24,16},{28,20},{1,9},{5... | collective-permute-start | bytes 393224 | tf_op jit(solution)/shard_map/ppermute | solution.py:24
  105.9 44.7 %copy-start.8 = (bf16[64,512]{1,0:T(8,128)(2,1)}, bf16[64,512]{1,0:T(8,128)(2,1)S(1)}, u32[]{:S(2)}) copy-start(bf16[64,512]{1,0:T(8,128)(2,1)S(1)} %collective-permute-done.45) | copy-start | bytes 196612
  105.9 9.5 %collective-permute-start.36 = (bf16[128,512]{1,0:T(8,128)(2,1)S(1)}, bf16[128,512]{1,0:T(8,128)(2,1)S(1)}, u32[]{:S(2)}, u32[]{:S(2)}) collective-permute-start(bf16[128,512]{1,0:T(8,128)(2,1)S(1)} %pad_maximum_fusion.23), channel_id=1, source_target_pairs={{0,8},{4,12},{8,0},{12,4},{16,24},{20,28},{24,16},{28,20},{1,9},{5... | collective-permute-start | bytes 393224 | tf_op jit(solution)/shard_map/ppermute | solution.py:24
  109.8 32.9 %copy-start.5 = (bf16[128,512]{1,0:T(8,128)(2,1)}, bf16[128,512]{1,0:T(8,128)(2,1)S(1)}, u32[]{:S(2)}) copy-start(bf16[128,512]{1,0:T(8,128)(2,1)S(1)} %collective-permute-done.8) | copy-start | bytes 393220
  109.8 7.2 %collective-permute-start.46 = (bf16[128,512]{1,0:T(8,128)(2,1)S(1)}, bf16[128,512]{1,0:T(8,128)(2,1)S(1)}, u32[]{:S(2)}, u32[]{:S(2)}) collective-permute-start(bf16[128,512]{1,0:T(8,128)(2,1)S(1)} %pad_maximum_fusion.24), channel_id=1, source_target_pairs={{0,8},{4,12},{8,0},{12,4},{16,24},{20,28},{24,16},{28,20},{1,9},{5... | collective-permute-start | bytes 393224 | tf_op jit(solution)/shard_map/ppermute | solution.py:24
  112.6 30.3 %copy-start.3 = (bf16[128,512]{1,0:T(8,128)(2,1)}, bf16[128,512]{1,0:T(8,128)(2,1)S(1)}, u32[]{:S(2)}) copy-start(bf16[128,512]{1,0:T(8,128)(2,1)S(1)} %collective-permute-done.26) | copy-start | bytes 393220
  112.6 6.7 %collective-permute-start.9 = (bf16[256,512]{1,0:T(8,128)(2,1)S(1)}, bf16[256,512]{1,0:T(8,128)(2,1)S(1)}, u32[]{:S(2)}, u32[]{:S(2)}) collective-permute-start(bf16[256,512]{1,0:T(8,128)(2,1)S(1)} %pad_maximum_fusion.17), channel_id=1, source_target_pairs={{0,4},{4,0},{8,12},{12,8},{16,20},{20,16},{24,28},{28,24},{1,5},{5... | collective-permute-start | bytes 786440 | tf_op jit(solution)/shard_map/ppermute | solution.py:24
  115.4 34.5 %copy-start.1 = (bf16[128,512]{1,0:T(8,128)(2,1)}, bf16[128,512]{1,0:T(8,128)(2,1)S(1)}, u32[]{:S(2)}) copy-start(bf16[128,512]{1,0:T(8,128)(2,1)S(1)} %collective-permute-done.36) | copy-start | bytes 393220
  115.4 8.0 %collective-permute-start.27 = (bf16[256,512]{1,0:T(8,128)(2,1)S(1)}, bf16[256,512]{1,0:T(8,128)(2,1)S(1)}, u32[]{:S(2)}, u32[]{:S(2)}) collective-permute-start(bf16[256,512]{1,0:T(8,128)(2,1)S(1)} %pad_maximum_fusion.18), channel_id=1, source_target_pairs={{0,2},{1,3},{2,0},{3,1},{4,6},{5,7},{6,4},{7,5},{8,10},{9,11},{10,... | collective-permute-start | bytes 786440 | tf_op jit(solution)/shard_map/ppermute | solution.py:24
  117.0 7.8 %collective-permute-start.37 = (bf16[256,512]{1,0:T(8,128)(2,1)S(1)}, bf16[256,512]{1,0:T(8,128)(2,1)S(1)}, u32[]{:S(2)}, u32[]{:S(2)}) collective-permute-start(bf16[256,512]{1,0:T(8,128)(2,1)S(1)} %pad_maximum_fusion.19), channel_id=1, source_target_pairs={{0,4},{4,0},{8,12},{12,8},{16,20},{20,16},{24,28},{28,24},{1,5},{5... | collective-permute-start | bytes 786440 | tf_op jit(solution)/shard_map/ppermute | solution.py:24
  119.4 9.7 %collective-permute-start.47 = (bf16[256,512]{1,0:T(8,128)(2,1)S(1)}, bf16[256,512]{1,0:T(8,128)(2,1)S(1)}, u32[]{:S(2)}, u32[]{:S(2)}) collective-permute-start(bf16[256,512]{1,0:T(8,128)(2,1)S(1)} %pad_maximum_fusion.20), channel_id=1, source_target_pairs={{0,2},{1,3},{2,0},{3,1},{4,6},{5,7},{6,4},{7,5},{8,10},{9,11},{10,... | collective-permute-start | bytes 786440 | tf_op jit(solution)/shard_map/ppermute | solution.py:24
  123.4 16.9 %collective-permute-start.10 = (bf16[512,512]{1,0:T(8,128)(2,1)S(1)}, bf16[512,512]{1,0:T(8,128)(2,1)S(1)}, u32[]{:S(2)}, u32[]{:S(2)}) collective-permute-start(bf16[512,512]{1,0:T(8,128)(2,1)S(1)} %pad_maximum_fusion.5), channel_id=1, source_target_pairs={{0,2},{1,3},{2,0},{3,1},{4,6},{5,7},{6,4},{7,5},{8,10},{9,11},{10,... | collective-permute-start | bytes 1572872 | tf_op jit(solution)/shard_map/ppermute | solution.py:24
  124.8 18.0 %collective-permute-start.28 = (bf16[256,1024]{1,0:T(8,128)(2,1)S(1)}, bf16[256,1024]{1,0:T(8,128)(2,1)S(1)}, u32[]{:S(2)}, u32[]{:S(2)}) collective-permute-start(bf16[256,1024]{1,0:T(8,128)(2,1)S(1)} %pad_maximum_fusion.12), channel_id=1, source_target_pairs={{0,4},{4,0},{8,12},{12,8},{16,20},{20,16},{24,28},{28,24},{1,5},{5... | collective-permute-start | bytes 1572872 | tf_op jit(solution)/shard_map/ppermute | solution.py:24
  129.0 20.9 %collective-permute-start.38 = (bf16[512,512]{1,0:T(8,128)(2,1)S(1)}, bf16[512,512]{1,0:T(8,128)(2,1)S(1)}, u32[]{:S(2)}, u32[]{:S(2)}) collective-permute-start(bf16[512,512]{1,0:T(8,128)(2,1)S(1)} %pad_maximum_fusion.13), channel_id=1, source_target_pairs={{0,2},{1,3},{2,0},{3,1},{4,6},{5,7},{6,4},{7,5},{8,10},{9,11},{10,... | collective-permute-start | bytes 1572872 | tf_op jit(solution)/shard_map/ppermute | solution.py:24
  130.4 19.6 %collective-permute-start.48 = (bf16[256,1024]{1,0:T(8,128)(2,1)S(1)}, bf16[256,1024]{1,0:T(8,128)(2,1)S(1)}, u32[]{:S(2)}, u32[]{:S(2)}) collective-permute-start(bf16[256,1024]{1,0:T(8,128)(2,1)S(1)} %pad_maximum_fusion.14), channel_id=1, source_target_pairs={{0,4},{4,0},{8,12},{12,8},{16,20},{20,16},{24,28},{28,24},{1,5},{5... | collective-permute-start | bytes 1572872 | tf_op jit(solution)/shard_map/ppermute | solution.py:24
  140.3 11.5 %collective-permute-start.14 = (f32[1,256]{1,0:T(1,128)S(1)}, f32[1,256]{1,0:T(1,128)S(1)}, u32[]{:S(2)}, u32[]{:S(2)}) collective-permute-start(f32[1,256]{1,0:T(1,128)S(1)} %bitcast.103), channel_id=1, source_target_pairs={{0,16},{4,20},{8,24},{12,28},{16,0},{20,4},{24,8},{28,12},{1,17},{... | collective-permute-start | bytes 3080 | tf_op jit(solution)/shard_map/ppermute | solution.py:24
  142.8 22.5 %collective-permute-start.11 = (bf16[512,1024]{1,0:T(8,128)(2,1)S(1)}, bf16[512,1024]{1,0:T(8,128)(2,1)}, u32[]{:S(2)}, u32[]{:S(2)}) collective-permute-start(bf16[512,1024]{1,0:T(8,128)(2,1)S(1)} %pad_maximum_fusion.1), channel_id=1, source_target_pairs={{0,1},{1,0},{2,3},{3,2},{4,5},{5,4},{6,7},{7,6},{8,9},{9,8},{10,11... | collective-permute-start | bytes 3145736 | tf_op jit(solution)/shard_map/ppermute | solution.py:24
  149.9 16.4 %collective-permute-start.29 = (bf16[512,1024]{1,0:T(8,128)(2,1)}, bf16[512,1024]{1,0:T(8,128)(2,1)}, u32[]{:S(2)}, u32[]{:S(2)}) collective-permute-start(bf16[512,1024]{1,0:T(8,128)(2,1)} %pad_maximum_fusion.2), channel_id=1, source_target_pairs={{0,1},{1,0},{2,3},{3,2},{4,5},{5,4},{6,7},{7,6},{8,9},{9,8},{10,11... | collective-permute-start | bytes 3145736 | tf_op jit(solution)/shard_map/ppermute | solution.py:24
  150.1 17.1 %collective-permute-start.39 = (bf16[512,1024]{1,0:T(8,128)(2,1)S(1)}, bf16[512,1024]{1,0:T(8,128)(2,1)}, u32[]{:S(2)}, u32[]{:S(2)}) collective-permute-start(bf16[512,1024]{1,0:T(8,128)(2,1)S(1)} %pad_maximum_fusion.3), channel_id=1, source_target_pairs={{0,1},{1,0},{2,3},{3,2},{4,5},{5,4},{6,7},{7,6},{8,9},{9,8},{10,11... | collective-permute-start | bytes 3145736 | tf_op jit(solution)/shard_map/ppermute | solution.py:24
  151.7 16.4 %collective-permute-start.49 = (bf16[512,1024]{1,0:T(8,128)(2,1)}, bf16[512,1024]{1,0:T(8,128)(2,1)}, u32[]{:S(2)}, u32[]{:S(2)}) collective-permute-start(bf16[512,1024]{1,0:T(8,128)(2,1)} %pad_maximum_fusion.4), channel_id=1, source_target_pairs={{0,1},{1,0},{2,3},{3,2},{4,5},{5,4},{6,7},{7,6},{8,9},{9,8},{10,11... | collective-permute-start | bytes 3145736 | tf_op jit(solution)/shard_map/ppermute | solution.py:24
  151.9 3.7 %collective-permute-start.15 = (f32[2,256]{1,0:T(2,128)S(1)}, f32[2,256]{1,0:T(2,128)S(1)}, u32[]{:S(2)}, u32[]{:S(2)}) collective-permute-start(f32[2,256]{1,0:T(2,128)S(1)} %pad_maximum_fusion.37), channel_id=1, source_target_pairs={{0,8},{4,12},{8,0},{12,4},{16,24},{20,28},{24,16},{28,20},{1,9},{5... | collective-permute-start | bytes 6152 | tf_op jit(solution)/shard_map/ppermute | solution.py:24
  156.1 4.0 %collective-permute-start.16 = (f32[4,256]{1,0:T(4,128)}, f32[4,256]{1,0:T(4,128)}, u32[]{:S(2)}, u32[]{:S(2)}) collective-permute-start(f32[4,256]{1,0:T(4,128)} %pad_maximum_fusion.36), channel_id=1, source_target_pairs={{0,4},{4,0},{8,12},{12,8},{16,20},{20,16},{24,28},{28,24},{1,5},{5... | collective-permute-start | bytes 12296 | tf_op jit(solution)/shard_map/ppermute | solution.py:24
  169.8 23.6 %collective-permute-start.55 = (bf16[256,128]{0,1:T(8,128)(2,1)S(1)}, bf16[256,128]{0,1:T(8,128)(2,1)S(1)}, u32[]{:S(2)}, u32[]{:S(2)}) collective-permute-start(bf16[256,128]{0,1:T(8,128)(2,1)S(1)} %multiply_convert_fusion.4), channel_id=1, source_target_pairs={{0,2},{1,3},{2,0},{3,1},{4,6},{5,7},{6,4},{7,5},{8,10},{9,11},{10,... | collective-permute-start | bytes 196616 | tf_op jit(solution)/shard_map/ppermute | solution.py:24
  177.0 16.8 %collective-permute-start.20 = (bf16[512,1024]{1,0:T(8,128)(2,1)S(1)}, bf16[512,1024]{1,0:T(8,128)(2,1)S(1)}, u32[]{:S(2)}, u32[]{:S(2)}) collective-permute-start(bf16[512,1024]{1,0:T(8,128)(2,1)S(1)} %convolution_convert_fusion.3), channel_id=1, source_target_pairs={{0,1},{1,0},{2,3},{3,2},{4,5},{5,4},{6,7},{7,6},{8,9},{9,8},{10,11... | collective-permute-start | bytes 3145736 | tf_op jit(solution)/shard_map/ppermute | solution.py:24
  182.3 12.6 %collective-permute-start.30 = (bf16[512,1024]{1,0:T(8,128)(2,1)S(1)}, bf16[512,1024]{1,0:T(8,128)(2,1)S(1)}, u32[]{:S(2)}, u32[]{:S(2)}) collective-permute-start(bf16[512,1024]{1,0:T(8,128)(2,1)S(1)} %convolution_convert_fusion.2), channel_id=1, source_target_pairs={{0,1},{1,0},{2,3},{3,2},{4,5},{5,4},{6,7},{7,6},{8,9},{9,8},{10,11... | collective-permute-start | bytes 3145736 | tf_op jit(solution)/shard_map/ppermute | solution.py:24
  187.8 9.1 %collective-permute-start.40 = (bf16[512,1024]{1,0:T(8,128)(2,1)S(1)}, bf16[512,1024]{1,0:T(8,128)(2,1)S(1)}, u32[]{:S(2)}, u32[]{:S(2)}) collective-permute-start(bf16[512,1024]{1,0:T(8,128)(2,1)S(1)} %convolution_convert_fusion.1), channel_id=1, source_target_pairs={{0,1},{1,0},{2,3},{3,2},{4,5},{5,4},{6,7},{7,6},{8,9},{9,8},{10,11... | collective-permute-start | bytes 3145736 | tf_op jit(solution)/shard_map/ppermute | solution.py:24
  192.8 6.1 %collective-permute-start.50 = (bf16[512,1024]{1,0:T(8,128)(2,1)S(1)}, bf16[512,1024]{1,0:T(8,128)(2,1)S(1)}, u32[]{:S(2)}, u32[]{:S(2)}) collective-permute-start(bf16[512,1024]{1,0:T(8,128)(2,1)S(1)} %convolution_convert_fusion), channel_id=1, source_target_pairs={{0,1},{1,0},{2,3},{3,2},{4,5},{5,4},{6,7},{7,6},{8,9},{9,8},{10,11... | collective-permute-start | bytes 3145736 | tf_op jit(solution)/shard_map/ppermute | solution.py:24
  193.5 54.1 %collective-permute-start.56 = (bf16[256,256]{0,1:T(8,128)(2,1)S(1)}, bf16[256,256]{0,1:T(8,128)(2,1)S(1)}, u32[]{:S(2)}, u32[]{:S(2)}) collective-permute-start(bf16[256,256]{0,1:T(8,128)(2,1)S(1)} %pad_maximum_fusion.25), channel_id=1, source_target_pairs={{0,1},{1,0},{2,3},{3,2},{4,5},{5,4},{6,7},{7,6},{8,9},{9,8},{10,11... | collective-permute-start | bytes 393224 | tf_op jit(solution)/shard_map/ppermute | solution.py:24
  194.3 14.9 %collective-permute-start.21 = (bf16[512,512]{1,0:T(8,128)(2,1)S(1)}, bf16[512,512]{1,0:T(8,128)(2,1)S(1)}, u32[]{:S(2)}, u32[]{:S(2)}) collective-permute-start(bf16[512,512]{1,0:T(8,128)(2,1)S(1)} %split.157), channel_id=1, source_target_pairs={{0,2},{1,3},{2,0},{3,1},{4,6},{5,7},{6,4},{7,5},{8,10},{9,11},{10,... | collective-permute-start | bytes 1572872 | tf_op jit(solution)/shard_map/ppermute | solution.py:24
  195.4 15.4 %collective-permute-start.31 = (bf16[256,1024]{1,0:T(8,128)(2,1)S(1)}, bf16[256,1024]{1,0:T(8,128)(2,1)S(1)}, u32[]{:S(2)}, u32[]{:S(2)}) collective-permute-start(bf16[256,1024]{1,0:T(8,128)(2,1)S(1)} %split.165), channel_id=1, source_target_pairs={{0,4},{4,0},{8,12},{12,8},{16,20},{20,16},{24,28},{28,24},{1,5},{5... | collective-permute-start | bytes 1572872 | tf_op jit(solution)/shard_map/ppermute | solution.py:24
  197.3 23.1 %collective-permute-start.41 = (bf16[512,512]{1,0:T(8,128)(2,1)S(1)}, bf16[512,512]{1,0:T(8,128)(2,1)S(1)}, u32[]{:S(2)}, u32[]{:S(2)}) collective-permute-start(bf16[512,512]{1,0:T(8,128)(2,1)S(1)} %split.173), channel_id=1, source_target_pairs={{0,2},{1,3},{2,0},{3,1},{4,6},{5,7},{6,4},{7,5},{8,10},{9,11},{10,... | collective-permute-start | bytes 1572872 | tf_op jit(solution)/shard_map/ppermute | solution.py:24
  199.4 22.7 %collective-permute-start.51 = (bf16[256,1024]{1,0:T(8,128)(2,1)S(1)}, bf16[256,1024]{1,0:T(8,128)(2,1)S(1)}, u32[]{:S(2)}, u32[]{:S(2)}) collective-permute-start(bf16[256,1024]{1,0:T(8,128)(2,1)S(1)} %split.181), channel_id=1, source_target_pairs={{0,4},{4,0},{8,12},{12,8},{16,20},{20,16},{24,28},{28,24},{1,5},{5... | collective-permute-start | bytes 1572872 | tf_op jit(solution)/shard_map/ppermute | solution.py:24
  209.4 17.8 %collective-permute-start.22 = (bf16[256,512]{1,0:T(8,128)(2,1)S(1)}, bf16[256,512]{1,0:T(8,128)(2,1)S(1)}, u32[]{:S(2)}, u32[]{:S(2)}) collective-permute-start(bf16[256,512]{1,0:T(8,128)(2,1)S(1)} %split.159), channel_id=1, source_target_pairs={{0,4},{4,0},{8,12},{12,8},{16,20},{20,16},{24,28},{28,24},{1,5},{5... | collective-permute-start | bytes 786440 | tf_op jit(solution)/shard_map/ppermute | solution.py:24
  211.0 16.4 %collective-permute-start.32 = (bf16[256,512]{1,0:T(8,128)(2,1)S(1)}, bf16[256,512]{1,0:T(8,128)(2,1)S(1)}, u32[]{:S(2)}, u32[]{:S(2)}) collective-permute-start(bf16[256,512]{1,0:T(8,128)(2,1)S(1)} %split.167), channel_id=1, source_target_pairs={{0,2},{1,3},{2,0},{3,1},{4,6},{5,7},{6,4},{7,5},{8,10},{9,11},{10,... | collective-permute-start | bytes 786440 | tf_op jit(solution)/shard_map/ppermute | solution.py:24
  220.6 11.1 %collective-permute-start.42 = (bf16[256,512]{1,0:T(8,128)(2,1)S(1)}, bf16[256,512]{1,0:T(8,128)(2,1)S(1)}, u32[]{:S(2)}, u32[]{:S(2)}) collective-permute-start(bf16[256,512]{1,0:T(8,128)(2,1)S(1)} %split.175), channel_id=1, source_target_pairs={{0,4},{4,0},{8,12},{12,8},{16,20},{20,16},{24,28},{28,24},{1,5},{5... | collective-permute-start | bytes 786440 | tf_op jit(solution)/shard_map/ppermute | solution.py:24
  222.3 9.8 %collective-permute-start.52 = (bf16[256,512]{1,0:T(8,128)(2,1)S(1)}, bf16[256,512]{1,0:T(8,128)(2,1)S(1)}, u32[]{:S(2)}, u32[]{:S(2)}) collective-permute-start(bf16[256,512]{1,0:T(8,128)(2,1)S(1)} %split.183), channel_id=1, source_target_pairs={{0,2},{1,3},{2,0},{3,1},{4,6},{5,7},{6,4},{7,5},{8,10},{9,11},{10,... | collective-permute-start | bytes 786440 | tf_op jit(solution)/shard_map/ppermute | solution.py:24
  227.2 6.9 %collective-permute-start.23 = (bf16[128,512]{1,0:T(8,128)(2,1)S(1)}, bf16[128,512]{1,0:T(8,128)(2,1)S(1)}, u32[]{:S(2)}, u32[]{:S(2)}) collective-permute-start(bf16[128,512]{1,0:T(8,128)(2,1)S(1)} %split.161), channel_id=1, source_target_pairs={{0,8},{4,12},{8,0},{12,4},{16,24},{20,28},{24,16},{28,20},{1,9},{5... | collective-permute-start | bytes 393224 | tf_op jit(solution)/shard_map/ppermute | solution.py:24
  227.6 6.7 %collective-permute-start.33 = (bf16[128,512]{1,0:T(8,128)(2,1)S(1)}, bf16[128,512]{1,0:T(8,128)(2,1)S(1)}, u32[]{:S(2)}, u32[]{:S(2)}) collective-permute-start(bf16[128,512]{1,0:T(8,128)(2,1)S(1)} %split.169), channel_id=1, source_target_pairs={{0,8},{4,12},{8,0},{12,4},{16,24},{20,28},{24,16},{28,20},{1,9},{5... | collective-permute-start | bytes 393224 | tf_op jit(solution)/shard_map/ppermute | solution.py:24
  231.8 8.1 %collective-permute-start.43 = (bf16[128,512]{1,0:T(8,128)(2,1)S(1)}, bf16[128,512]{1,0:T(8,128)(2,1)S(1)}, u32[]{:S(2)}, u32[]{:S(2)}) collective-permute-start(bf16[128,512]{1,0:T(8,128)(2,1)S(1)} %split.177), channel_id=1, source_target_pairs={{0,8},{4,12},{8,0},{12,4},{16,24},{20,28},{24,16},{28,20},{1,9},{5... | collective-permute-start | bytes 393224 | tf_op jit(solution)/shard_map/ppermute | solution.py:24
  232.2 9.3 %collective-permute-start.53 = (bf16[128,512]{1,0:T(8,128)(2,1)S(1)}, bf16[128,512]{1,0:T(8,128)(2,1)S(1)}, u32[]{:S(2)}, u32[]{:S(2)}) collective-permute-start(bf16[128,512]{1,0:T(8,128)(2,1)S(1)} %split.185), channel_id=1, source_target_pairs={{0,8},{4,12},{8,0},{12,4},{16,24},{20,28},{24,16},{28,20},{1,9},{5... | collective-permute-start | bytes 393224 | tf_op jit(solution)/shard_map/ppermute | solution.py:24
  234.2 9.1 %collective-permute-start.24 = (bf16[64,512]{1,0:T(8,128)(2,1)S(1)}, bf16[64,512]{1,0:T(8,128)(2,1)S(1)}, u32[]{:S(2)}, u32[]{:S(2)}) collective-permute-start(bf16[64,512]{1,0:T(8,128)(2,1)S(1)} %split.163), channel_id=1, source_target_pairs={{0,16},{4,20},{8,24},{12,28},{16,0},{20,4},{24,8},{28,12},{1,17},{... | collective-permute-start | bytes 196616 | tf_op jit(solution)/shard_map/ppermute | solution.py:24
  234.3 11.1 %collective-permute-start.34 = (bf16[64,512]{1,0:T(8,128)(2,1)S(1)}, bf16[64,512]{1,0:T(8,128)(2,1)S(1)}, u32[]{:S(2)}, u32[]{:S(2)}) collective-permute-start(bf16[64,512]{1,0:T(8,128)(2,1)S(1)} %split.171), channel_id=1, source_target_pairs={{0,16},{4,20},{8,24},{12,28},{16,0},{20,4},{24,8},{28,12},{1,17},{... | collective-permute-start | bytes 196616 | tf_op jit(solution)/shard_map/ppermute | solution.py:24
  240.0 7.0 %collective-permute-start.44 = (bf16[64,512]{1,0:T(8,128)(2,1)S(1)}, bf16[64,512]{1,0:T(8,128)(2,1)S(1)}, u32[]{:S(2)}, u32[]{:S(2)}) collective-permute-start(bf16[64,512]{1,0:T(8,128)(2,1)S(1)} %split.179), channel_id=1, source_target_pairs={{0,16},{4,20},{8,24},{12,28},{16,0},{20,4},{24,8},{28,12},{1,17},{... | collective-permute-start | bytes 196616 | tf_op jit(solution)/shard_map/ppermute | solution.py:24
  241.6 6.0 %collective-permute-start.54 = (bf16[64,512]{1,0:T(8,128)(2,1)S(1)}, bf16[64,512]{1,0:T(8,128)(2,1)S(1)}, u32[]{:S(2)}, u32[]{:S(2)}) collective-permute-start(bf16[64,512]{1,0:T(8,128)(2,1)S(1)} %split.187), channel_id=1, source_target_pairs={{0,16},{4,20},{8,24},{12,28},{16,0},{20,4},{24,8},{28,12},{1,17},{... | collective-permute-start | bytes 196616 | tf_op jit(solution)/shard_map/ppermute | solution.py:24
  (65 other events, 378.5 us)
where the time goes:
time: 254 us; the launch traced here: 249 us
  waiting for transfers between devices  86.1 us (34%)
  starting transfers between devices  71.5 us (28%)
  matrix products  53.2 us (21%)
  local copies, waits for them, and re-layouts  23.2 us (9%)
  other arithmetic  12.9 us (5%)
    ppermute x57, waiting for transfers between devices, from_partner(): return lax.ppermute(value, axis, pairs)  86.1 us
    ppermute x57, starting transfers between devices, from_partner(): return lax.ppermute(value, axis, pairs)  71.5 us
    dot_general x20, matrix products, dot_halves(): jnp.dot(half, part, preferred_element_type=jnp.float32)  19.6 us
    dot_general x1, matrix products, attention_heads(): jnp.einsum('nthd,nhdv->nthv', query_decay, states[:block_count], precisio...  11.9 us
    dot_general x1, matrix products, attention_heads(): jnp.einsum('nmhd,mhdv->nhdv', jnp.exp(span_logs), update, precision=HIGHEST)  6.12 us
    slice x8, local copies, waits for them, and re-layouts, dense_experts(): own_halves.append([half[:rows] for half in halves])  5.59 us
    dynamic_slice x4, local copies, waits for them, and re-layouts, relative_rows(): lax.dynamic_slice_in_dim(matrix, (place ^ mask) * height, height, 0)  5.45 us
    concatenate x24, other arithmetic, spread(): value = jnp.concatenate([value, arrived], 0 if axis == 'sp' else 1)  5.19 us
  transfers between devices with their start and end apart: 57, of which 26 were waited for; matrix products, arithmetic and copies ran while one was open for 25% of the time, Pallas kernels for 0%

commit v1 on v0

--- a/solution.py
+++ b/solution.py
@@ -1,6 +1,10 @@
+import functools
+
 import jax
 import jax.numpy as jnp
 from jax import lax
+from jax.experimental import pallas as pl
+from jax.experimental.pallas import tpu as pltpu
 from jax.sharding import PartitionSpec as P
 
 DK = 128
@@ -178,6 +182,647 @@
     return (mid_float + routed + shared_out).astype(jnp.bfloat16)
 
 
+SLAB_HALF = 256
+EXPERT_PARTS = 3
+
+
+def remote(source, target, send_sem, recv_sem, device):
+    return pltpu.make_async_remote_copy(
+        src_ref=source,
+        dst_ref=target,
+        send_sem=send_sem,
+        recv_sem=recv_sem,
+        device_id=device,
+        device_id_type=pl.DeviceIdType.MESH,
+    )
+
+
+def swish(value):
+    return value / (1.0 + jnp.exp(-value))
+
+
+def exchange_kernel(
+    most,
+    mid_ref,
+    gain_ref,
+    table_ref,
+    gate_hbm,
+    up_hbm,
+    down_hbm,
+    shared_gate_hbm,
+    shared_up_hbm,
+    shared_down_hbm,
+    out_ref,
+    gate_ref,
+    up_ref,
+    down_ref,
+    shared_gate_ref,
+    shared_up_ref,
+    shared_down_ref,
+    tables,
+    ranks,
+    slot_weights,
+    picks,
+    own_rows,
+    partner_high,
+    core_rows,
+    line_rows,
+    side_out,
+    expert_rows,
+    hidden_rows,
+    core_out,
+    core_in,
+    kept_rows,
+    y_out,
+    y_in,
+    results,
+    side_in,
+    line_out,
+    left_in,
+    right_in,
+    last_out,
+    last_in,
+    shared_hidden,
+    routed,
+    base,
+    weight_sem,
+    table_send,
+    table_recv,
+    own_send,
+    own_recv,
+    core_send,
+    core_recv,
+    left_send,
+    right_send,
+    line_recv,
+    side_send,
+    side_recv,
+    y_send,
+    y_recv,
+    pair_send,
+    pair_recv,
+    back_core_send,
+    back_core_recv,
+    back_y_send,
+    back_y_recv,
+    back_side_send,
+    back_side_recv,
+    back_line_send,
+    left_recv,
+    right_recv,
+    shared_send,
+    shared_recv,
+    last_send,
+    last_recv,
+):
+    bf16, f32 = jnp.bfloat16, jnp.float32
+    sp_count, tp_count = lax.axis_size("sp"), lax.axis_size("tp")
+    depth = sp_count // 2
+    tokens = mid_ref.shape[0]
+    half = mid_ref.shape[1] // 2
+    parts = 2 * tp_count
+    width = half * parts
+    sp, tp = lax.axis_index("sp"), lax.axis_index("tp")
+    z, x = sp // 2, sp % 2
+    y, core = tp // 2, tp % 2
+    tp_y = (1 - y) * 2 + core
+    tp_core = y * 2 + (1 - core)
+    side = (z * 2 + 1 - x, tp)
+    over_y = (sp, tp_y)
+    over_core = (sp, tp_core)
+    left, right = (sp - 2, tp), (sp + 2, tp)
+    has_left, has_right = z > 0, z < depth - 1
+    pending = []
+
+    def begin(copy, when=None):
+        if when is None:
+            copy.start()
+        else:
+            pl.when(when)(copy.start)
+        pending.append((copy, when))
+
+    def arrive(target, sem):
+        remote(target, target, weight_sem.at[0], sem, (sp, tp)).wait_recv()
+
+    order = [
+        z,
+        jnp.where(z == 0, 1, jnp.where(z == 1, 0, jnp.where(z == 2, 3, 2))),
+        jnp.where(z == 0, 2, jnp.where(z == 1, 2, jnp.where(z == 2, 1, 1))),
+        jnp.where(z == 0, 3, jnp.where(z == 1, 3, 0)),
+    ]
+    back_order = [
+        jnp.where(z == 0, 1, jnp.where(z == 1, 2, jnp.where(z == 2, 1, 2))),
+        jnp.where(z == 0, 2, jnp.where(z == 1, 3, jnp.where(z == 2, 0, 1))),
+        jnp.where(z == 0, 3, jnp.where(z == 1, 0, jnp.where(z == 2, 3, 0))),
+        z,
+    ]
+
+    barrier = pltpu.get_barrier_semaphore()
+    peers = [(lax.rem(sp + step, sp_count), tp) for step in range(1, sp_count)]
+    peers += [(sp, lax.rem(tp + step, tp_count)) for step in range(1, tp_count)]
+    for peer in peers:
+        pl.semaphore_signal(barrier, inc=1, device_id=peer, device_id_type=pl.DeviceIdType.MESH)
+    weights = [
+        (gate_hbm, gate_ref),
+        (up_hbm, up_ref),
+        (down_hbm, down_ref),
+        (shared_gate_hbm, shared_gate_ref),
+        (shared_up_hbm, shared_up_ref),
+        (shared_down_hbm, shared_down_ref),
+    ]
+    loads = [
+        pltpu.make_async_copy(hbm, vmem, weight_sem.at[number + 1])
+        for number, (hbm, vmem) in enumerate(weights)
+    ]
+    for load in loads:
+        load.start()
+    pl.semaphore_wait(barrier, len(peers))
+
+    low, high = mid_ref.at[:, pl.ds(0, half)], mid_ref.at[:, pl.ds(half, half)]
+    for step in range(1, sp_count):
+        peer = lax.rem(sp + step, sp_count)
+        begin(
+            remote(table_ref, tables.at[sp], table_send.at[step], table_recv.at[sp], (peer, tp))
+        )
+    begin(remote(low, line_rows.at[z, 2], own_send.at[0], own_recv.at[0], over_y))
+    for part, source in ((0, high), (1, low)):
+        target = line_rows.at[z, part]
+        begin(remote(source, target, left_send.at[z, part], line_recv.at[z, part], left), has_left)
+        begin(
+            remote(source, target, right_send.at[z, part], line_recv.at[z, part], right), has_right
+        )
+    begin(remote(high, partner_high, own_send.at[1], own_recv.at[1], over_y))
+    begin(remote(low, core_rows.at[0], core_send.at[0], core_recv.at[0], over_core))
+    begin(remote(high, core_rows.at[1], core_send.at[1], core_recv.at[1], over_core))
+    own_rows[0] = mid_ref[:, half:]
+    own_rows[1] = mid_ref[:, :half]
+    tables[sp] = table_ref[...]
+
+    earlier = (
+        lax.broadcasted_iota(jnp.int32, (tokens, tokens), 0)
+        < lax.broadcasted_iota(jnp.int32, (tokens, tokens), 1)
+    ).astype(f32).astype(bf16)
+    slots = lax.broadcasted_iota(jnp.int32, (most, tokens), 0).astype(f32)
+
+    def rank_block(source):
+        chosen = tables[source] > 0.0
+        counts = jnp.dot(
+            jnp.where(chosen, 1.0, 0.0).astype(bf16), earlier, preferred_element_type=f32
+        )
+        ranks[source] = jnp.where(chosen, counts, -1.0)
+
+    def pick(source, expert):
+        return slots == ranks[source, pl.ds(expert, 1), :]
+
+    def slot_block(source):
+        weight = jnp.where(pick(source, sp), tables[source, pl.ds(sp, 1), :], 0.0)
+        slot_weights[source] = jnp.broadcast_to(
+            jnp.sum(weight, axis=1, keepdims=True), (most, 128)
+        )
+
+    def pick_block(depth_at):
+        source = depth_at * 2 + x
+        for number, expert in ((0, sp), (1, z * 2 + 1 - x)):
+            picks[depth_at, pl.ds(number * most, most), :] = (
+                jnp.where(pick(source, expert), 1.0, 0.0).astype(bf16)
+            )
+
+    def prepare(depth_at, first):
+        for source in (depth_at * 2 + x, depth_at * 2 + 1 - x):
+            if first:
+                @pl.when(source != sp)
+                def _():
+                    arrive(tables.at[source], table_recv.at[source])
+            else:
+                arrive(tables.at[source], table_recv.at[source])
+            rank_block(source)
+            slot_block(source)
+        pick_block(depth_at)
+
+    prepare(order[0], True)
+    arrive(line_rows.at[z, 2], own_recv.at[0])
+    target = line_rows.at[z, 2]
+    begin(remote(target, target, left_send.at[z, 2], line_recv.at[z, 2], left), has_left)
+    begin(remote(target, target, right_send.at[z, 2], line_recv.at[z, 2], right), has_right)
+    begin(remote(target, core_rows.at[2], core_send.at[2], core_recv.at[2], over_core))
+
+    held = (tp * 2 + 1, tp * 2, tp_y * 2)
+    late = tp_y * 2 + 1
+
+    def to_core(number, source):
+        ref = expert_rows.at[number, source]
+        begin(
+            remote(ref, ref, pair_send.at[number, source], pair_recv.at[number, source], over_core)
+        )
+
+    def to_y(source):
+        ref = expert_rows.at[held[0], source]
+        begin(remote(ref, ref, y_send.at[source], y_recv.at[source], over_y))
+
+    def lines(k):
+        at = order[k]
+        source = at * 2 + x
+        for part in range(EXPERT_PARTS):
+            if k > 0:
+                ref = line_rows.at[at, part]
+                arrive(ref, line_recv.at[at, part])
+                begin(
+                    remote(ref, ref, left_send.at[at, part], line_recv.at[at, part], left),
+                    jnp.logical_and(at > z, has_left),
+                )
+                begin(
+                    remote(ref, ref, right_send.at[at, part], line_recv.at[at, part], right),
+                    jnp.logical_and(at < z, has_right),
+                )
+                rows = line_rows[at, part]
+            else:
+                rows = line_rows[z, 2] if part == 2 else own_rows[part]
+            chosen = jnp.dot(picks[at], rows, preferred_element_type=f32).astype(bf16)
+            side_out[at, part] = chosen[most:]
+            begin(
+                remote(
+                    side_out.at[at, part],
+                    expert_rows.at[held[part], source],
+                    side_send.at[at, part],
+                    side_recv.at[at, part],
+                    side,
+                )
+            )
+            expert_rows[held[part], source] = chosen[:most]
+            if part == 0 and k > 0:
+                to_y(source)
+            to_core(held[part], source)
+        if k == 0:
+            arrive(partner_high, own_recv.at[1])
+            begin(remote(partner_high, core_rows.at[3], core_send.at[3], core_recv.at[3], over_core))
+            expert_rows[late, source] = jnp.dot(
+                picks[at, pl.ds(0, most), :], partner_high[...], preferred_element_type=f32
+            ).astype(bf16)
+            to_core(late, source)
+
+    def sides(k):
+        at = order[k]
+        source = at * 2 + 1 - x
+        for part in range(EXPERT_PARTS):
+            arrive(expert_rows.at[held[part], source], side_recv.at[at, part])
+            if part == 0:
+                to_y(source)
+            to_core(held[part], source)
+
+    def lates(k, which):
+        at = order[k]
+        source = at * 2 + (x if which == 0 else 1 - x)
+        arrive(expert_rows.at[late, source], y_recv.at[source])
+        to_core(late, source)
+
+    other_held = (tp_core * 2 + 1, tp_core * 2, ((1 - y) * 2 + 1 - core) * 2)
+    other_late = ((1 - y) * 2 + 1 - core) * 2 + 1
+
+    def experts(k):
+        for which in range(2):
+            source = order[k] * 2 + (x if which == 0 else 1 - x)
+            for number in (*other_held, other_late):
+                arrive(expert_rows.at[number, source], pair_recv.at[number, source])
+            pieces, squares = [], None
+            for number in range(parts):
+                rows = expert_rows[number, source]
+                pieces.append(rows * gain_ref[pl.ds(number, 1), :].astype(bf16))
+                wide = rows.astype(f32)
+                squares = wide * wide if squares is None else squares + wide * wide
+            inverse = lax.rsqrt(jnp.sum(squares, axis=1, keepdims=True) / width + EPSILON)
+            joined = jnp.concatenate(pieces, axis=1)
+            gate = jnp.dot(joined, gate_ref[...], preferred_element_type=f32) * inverse
+            up = jnp.dot(joined, up_ref[...], preferred_element_type=f32) * inverse
+            hidden = (swish(gate) * up * slot_weights[source][:, :1]).astype(bf16)
+            hidden_rows[source] = hidden
+            for number, row in ((0, y), (1, 1 - y)):
+                slab = (row * 2 + 1 - core) * (2 * half)
+                block = down_ref[:, pl.ds(pl.multiple_of(slab, 2 * half), 2 * half)]
+                core_out[source, number] = jnp.dot(
+                    hidden, block, preferred_element_type=f32
+                ).astype(bf16)
+            begin(
+                remote(
+                    core_out.at[source],
+                    core_in.at[source],
+                    back_core_send.at[source],
+                    back_core_recv.at[source],
+                    over_core,
+                )
+            )
+
+    def pairs(k):
+        for which in range(2):
+            source = order[k] * 2 + (x if which == 0 else 1 - x)
+            arrive(core_in.at[source], back_core_recv.at[source])
+            hidden = hidden_rows[source]
+
+            def summed(number, row):
+                slab = (row * 2 + core) * (2 * half)
+                block = down_ref[:, pl.ds(pl.multiple_of(slab, 2 * half), 2 * half)]
+                return jnp.dot(hidden, block, preferred_element_type=f32) + core_in[
+                    source, number
+                ].astype(f32)
+
+            other = summed(1, 1 - y)
+            y_out[source] = other[:, half:].astype(bf16)
+            begin(
+                remote(
+                    y_out.at[source],
+                    y_in.at[source],
+                    back_y_send.at[source],
+                    back_y_recv.at[source],
+                    over_y,
+                )
+            )
+            results[source, 2] = other[:, :half].astype(bf16)
+            mine = summed(0, y)
+            results[source, 1] = mine[:, :half].astype(bf16)
+            kept_rows[source] = mine[:, half:]
+
+    def ready(k):
+        at = order[k]
+        for which in (1, 0):
+            source = at * 2 + (x if which == 0 else 1 - x)
+            if which == 1:
+                for part in (2, 1):
+                    give_side(at, source, part)
+            arrive(y_in.at[source], back_y_recv.at[source])
+            results[source, 0] = (kept_rows[source] + y_in[source].astype(f32)).astype(bf16)
+            if which == 1:
+                give_side(at, source, 0)
+
+    def give_side(at, source, part):
+        begin(
+            remote(
+                results.at[source, part],
+                side_in.at[at, part],
+                back_side_send.at[at, part],
+                back_side_recv.at[at, part],
+                side,
+            )
+        )
+
+    def spread_back(at, part):
+        arrive(side_in.at[at, part], back_side_recv.at[at, part])
+        rows = jnp.concatenate([results[at * 2 + x, part], side_in[at, part]], axis=0)
+        return lax.dot_general(
+            picks[at], rows, (((0,), (0,)), ((), ())), preferred_element_type=f32
+        )
+
+    def arrived(at, part):
+        from_right = jnp.logical_and(at <= z, has_right)
+        from_left = jnp.logical_and(at >= z, has_left)
+
+        @pl.when(from_right)
+        def _():
+            arrive(right_in.at[at, part], right_recv.at[at, part])
+
+        @pl.when(from_left)
+        def _():
+            arrive(left_in.at[at, part], left_recv.at[at, part])
+
+        return jnp.where(from_right, right_in[at, part].astype(f32), 0.0) + jnp.where(
+            from_left, left_in[at, part].astype(f32), 0.0
+        )
+
+    def back_lines(k):
+        at = back_order[k]
+        for part in (2, 1, 0):
+            routed[part] = spread_back(at, part) + arrived(at, part)
+            line_out[at, part] = routed[part].astype(bf16)
+            source = line_out.at[at, part]
+            begin(
+                remote(
+                    source,
+                    right_in.at[at, part],
+                    back_line_send.at[at, part],
+                    right_recv.at[at, part],
+                    left,
+                ),
+                at < z,
+            )
+            begin(
+                remote(
+                    source,
+                    left_in.at[at, part],
+                    back_line_send.at[at, part],
+                    left_recv.at[at, part],
+                    right,
+                ),
+                at > z,
+            )
+
+    def own_lines(part):
+        routed[part] = spread_back(z, part) + arrived(z, part)
+
+    def shared_first():
+        for number in range(4):
+            arrive(core_rows.at[number], core_recv.at[number])
+        blocks = [
+            (own_rows[1], tp * 2),
+            (own_rows[0], tp * 2 + 1),
+            (line_rows[z, 2], tp_y * 2),
+            (partner_high[...], tp_y * 2 + 1),
+            (core_rows[0], tp_core * 2),
+            (core_rows[1], tp_core * 2 + 1),
+            (core_rows[2], other_held[2]),
+            (core_rows[3], other_late),
+        ]
+        squares = gate = up = 0.0
+        for rows, number in blocks:
+            wide = rows.astype(f32)
+            squares = squares + wide * wide
+            scaled = rows * gain_ref[pl.ds(number, 1), :].astype(bf16)
+            span = pl.ds(pl.multiple_of(number * half, half), half)
+            gate = gate + jnp.dot(scaled, shared_gate_ref[span, :], preferred_element_type=f32)
+            up = up + jnp.dot(scaled, shared_up_ref[span, :], preferred_element_type=f32)
+        inverse = lax.rsqrt(jnp.sum(squares, axis=1, keepdims=True) / width + EPSILON)
+        shared_hidden[tp] = (swish(gate * inverse) * (up * inverse)).astype(bf16)
+        for step in range(1, tp_count):
+            peer = lax.rem(tp + step, tp_count)
+            begin(
+                remote(
+                    shared_hidden.at[tp],
+                    shared_hidden.at[tp],
+                    shared_send.at[step],
+                    shared_recv.at[tp],
+                    (sp, peer),
+                )
+            )
+
+    def shared_second():
+        for step in range(1, tp_count):
+            peer = lax.rem(tp + step, tp_count)
+            arrive(shared_hidden.at[peer], shared_recv.at[peer])
+        joined = jnp.concatenate([shared_hidden[number] for number in range(tp_count)], axis=1)
+        base[...] = mid_ref[...].astype(f32) + jnp.dot(
+            joined, shared_down_ref[...], preferred_element_type=f32
+        )
+
+    lines(0)
+    for k in range(1, depth):
+        prepare(order[k], False)
+    for load in loads:
+        load.wait()
+    sides(0)
+    shared_first()
+    lines(1)
+    lates(0, 1)
+    experts(0)
+    sides(1)
+    lines(2)
+    lates(1, 0)
+    lates(1, 1)
+    experts(1)
+    pairs(0)
+    sides(2)
+    lines(3)
+    lates(2, 0)
+    lates(2, 1)
+    experts(2)
+    pairs(1)
+    ready(0)
+    sides(3)
+    lates(3, 0)
+    lates(3, 1)
+    experts(3)
+    pairs(2)
+    ready(1)
+    pairs(3)
+    ready(2)
+    back_lines(0)
+    ready(3)
+    back_lines(1)
+    back_lines(2)
+    shared_second()
+    own_lines(2)
+    last_out[...] = routed[2].astype(bf16)
+    begin(remote(last_out, last_in, last_send, last_recv, over_y))
+    own_lines(1)
+    own_lines(0)
+    out_ref[:, half:] = (base[:, half:] + routed[0]).astype(bf16)
+    arrive(last_in, last_recv)
+    out_ref[:, :half] = (base[:, :half] + routed[1] + last_in[...].astype(f32)).astype(bf16)
+    for copy, when in pending:
+        if when is None:
+            copy.wait_send()
+        else:
+            pl.when(when)(copy.wait_send)
+
+
+def exchange_experts(
+    mid_local,
+    feedforward_gain,
+    routing,
+    router_score,
+    expert_gate_weight,
+    expert_up_weight,
+    expert_down_weight,
+    shared_expert_gate,
+    shared_expert_up,
+    shared_expert_down,
+):
+    sp_count, tp_count = lax.axis_size("sp"), lax.axis_size("tp")
+    depth = sp_count // 2
+    tokens, slab = mid_local.shape
+    half = slab // 2
+    parts = 2 * tp_count
+    picked = routing.shape[1]
+    most = 3 * tokens * picked // (2 * sp_count)
+    route_weight = ROUTE_SCALE * router_score / jnp.sum(router_score, axis=1, keepdims=True)
+    expert_ids = jnp.arange(sp_count, dtype=jnp.int32)
+    table = jnp.sum(
+        jnp.where(
+            routing.T[None, :, :] == expert_ids[:, None, None], route_weight.T[None, :, :], 0.0
+        ),
+        axis=1,
+    )
+    gain = feedforward_gain.astype(jnp.float32).reshape(parts, half)
+    bf16, f32 = jnp.bfloat16, jnp.float32
+    vmem = pltpu.VMEM
+    dma = pltpu.SemaphoreType.DMA
+    hidden_width = expert_gate_weight.shape[1]
+    in_vmem = pl.BlockSpec(memory_space=pltpu.VMEM)
+    in_any = pl.BlockSpec(memory_space=pl.ANY)
+    weights = (
+        expert_gate_weight,
+        expert_up_weight,
+        expert_down_weight,
+        shared_expert_gate,
+        shared_expert_up,
+        shared_expert_down,
+    )
+    return pl.pallas_call(
+        functools.partial(exchange_kernel, most),
+        name="exchange_experts",
+        out_shape=jax.ShapeDtypeStruct(mid_local.shape, bf16),
+        in_specs=[in_vmem] * 3 + [in_any] * len(weights),
+        out_specs=in_vmem,
+        scratch_shapes=[vmem(weight.shape, bf16) for weight in weights]
+        + [
+            vmem((sp_count, sp_count, tokens), f32),
+            vmem((sp_count, sp_count, tokens), f32),
+            vmem((sp_count, most, 128), f32),
+            vmem((depth, 2 * most, tokens), bf16),
+            vmem((2, tokens, half), bf16),
+            vmem((tokens, half), bf16),
+            vmem((4, tokens, half), bf16),
+            vmem((depth, EXPERT_PARTS, tokens, half), bf16),
+            vmem((depth, EXPERT_PARTS, most, half), bf16),
+            vmem((parts, sp_count, most, half), bf16),
+            vmem((sp_count, most, hidden_width), bf16),
+            vmem((sp_count, 2, most, slab), bf16),
+            vmem((sp_count, 2, most, slab), bf16),
+            vmem((sp_count, most, half), f32),
+            vmem((sp_count, most, half), bf16),
+            vmem((sp_count, most, half), bf16),
+            vmem((sp_count, EXPERT_PARTS, most, half), bf16),
+            vmem((depth, EXPERT_PARTS, most, half), bf16),
+            vmem((depth, EXPERT_PARTS, tokens, half), bf16),
+            vmem((depth, EXPERT_PARTS, tokens, half), bf16),
+            vmem((depth, EXPERT_PARTS, tokens, half), bf16),
+            vmem((tokens, half), bf16),
+            vmem((tokens, half), bf16),
+            vmem((tp_count, tokens, shared_expert_gate.shape[1]), bf16),
+            vmem((EXPERT_PARTS, tokens, half), f32),
+            vmem((tokens, slab), f32),
+            dma((len(weights) + 1,)),
+            dma((sp_count,)),
+            dma((sp_count,)),
+            dma((2,)),
+            dma((2,)),
+            dma((4,)),
+            dma((4,)),
+            dma((depth, EXPERT_PARTS)),
+            dma((depth, EXPERT_PARTS)),
+            dma((depth, EXPERT_PARTS)),
+            dma((depth, EXPERT_PARTS)),
+            dma((depth, EXPERT_PARTS)),
+            dma((sp_count,)),
+            dma((sp_count,)),
+            dma((parts, sp_count)),
+            dma((parts, sp_count)),
+            dma((sp_count,)),
+            dma((sp_count,)),
+            dma((sp_count,)),
+            dma((sp_count,)),
+            dma((depth, EXPERT_PARTS)),
+            dma((depth, EXPERT_PARTS)),
+            dma((depth, EXPERT_PARTS)),
+            dma((depth, EXPERT_PARTS)),
+            dma((depth, EXPERT_PARTS)),
+            dma((tp_count,)),
+            dma((tp_count,)),
+            dma,
+            dma,
+        ],
+        compiler_params=pltpu.CompilerParams(
+            collective_id=1, has_side_effects=True, vmem_limit_bytes=60 * 1024 * 1024
+        ),
+    )(mid_local, gain, table, *weights)
+
+
 def attention_heads(queries, key_matrix, value_matrix, decay_preactivation, extra_log_decay):
     tokens = queries.shape[0]
     local_head_count = extra_log_decay.shape[1]
@@ -279,8 +924,8 @@
     )
     mid_local = (residual.astype(jnp.float32) + projected).astype(jnp.bfloat16)
     most = 3 * tokens * routing.shape[1] // (2 * lax.axis_size("sp"))
-    if lax.axis_size("tp") == FF_PARTS and 2 * most >= tokens:
-        return dense_experts(
+    if lax.axis_size("tp") == FF_PARTS and lax.axis_size("sp") == 8:
+        return exchange_experts(
             mid_local,
             feedforward_gain,
             routing,

time: 254 us -> 184 us (0.72); the launches traced: 249 us -> 183 us
  Pallas kernels: 0 us -> 116 us
  waiting for transfers between devices: 86.1 us -> 19.1 us
  starting transfers between devices: 71.5 us -> 12.9 us
  matrix products: 53.2 us -> 16.7 us
  local copies, waits for them, and re-layouts: 23.2 us -> 11.8 us
  other arithmetic: 12.9 us -> 6.42 us
    pallas_call x0 -> x1, Pallas kernels: none -> 116 us  [exchange_experts(): pl.pallas_call(functools.partial(exchange_kernel, most), name='exchange_e...]
    ppermute x57 -> x7, waiting for transfers between devices: 86.1 us -> 19.1 us  [from_partner(): return lax.ppermute(value, axis, pairs)]
    ppermute x57 -> x7, starting transfers between devices: 71.5 us -> 12.9 us  [from_partner(): return lax.ppermute(value, axis, pairs)]
    dot_general x29 -> x0, matrix products: 24.1 us -> none  [the longest x20 19.6 us: dot_halves(): jnp.dot(half, part, preferred_element_type=jnp.float32)]
    dot_general x1, matrix products: 11.9 us -> 1.75 us  [attention_heads(): jnp.einsum('nthd,nhdv->nthv', query_decay, states[:block_count], precisio...]
    slice x11 -> x0, local copies, waits for them, and re-layouts: 5.75 us -> none  [the longest x8 5.59 us: dense_experts(): own_halves.append([half[:rows] for half in halves])]
    concatenate x24 -> x1, other arithmetic: 5.19 us -> 0.08 us  [spread(): value = jnp.concatenate([value, arrived], 0 if axis == 'sp' else 1)]
    mul x8 -> x0, local copies, waits for them, and re-layouts: 3.32 us -> none  [the longest x4 2.49 us: dense_experts(): jax.nn.silu(dot_halves(halves, gate) * row_inverse)]
  transfers between devices with their start and end apart: 57 -> 7, of which waited for: 26 -> 4; matrix products, arithmetic and copies ran while one was open for 25% -> 12% of each run, Pallas kernels for 0% -> 0%
where the time goes in v1:
time: 184 us; the launch traced here: 183 us
  Pallas kernels  116 us (63%)
  waiting for transfers between devices  19.1 us (10%)
  matrix products  16.7 us (9%)
  starting transfers between devices  12.9 us (7%)
  local copies, waits for them, and re-layouts  11.8 us (6%)
  other arithmetic  6.42 us (3%)
    pallas_call x1, Pallas kernels, exchange_experts(): pl.pallas_call(functools.partial(exchange_kernel, most), name='exchange_e...  116 us
    ppermute x7, waiting for transfers between devices, from_partner(): return lax.ppermute(value, axis, pairs)  19.1 us
    ppermute x7, starting transfers between devices, from_partner(): return lax.ppermute(value, axis, pairs)  12.9 us
    dot_general x1, matrix products, attention_heads(): jnp.einsum('nmhd,mhdv->nhdv', jnp.exp(span_logs), update, precision=HIGHEST)  6.09 us
  transfers between devices with their start and end apart: 7, of which 4 were waited for; matrix products, arithmetic and copies ran while one was open for 12% of the time, Pallas kernels for 0%

profile of v1, /device:TPU:0, one launch (start us, length us, event | category | flops | bytes accessed | tf_op | source)
XLA Modules:
  0.0 183.2 jit_solution(12883735576274605099)
XLA Ops:
  0.0 0.0 copy-start.2
  0.0 0.9 copy.84
  0.9 1.3 fusion.37
  2.2 0.2 div.29
  2.4 0.3 fusion.47
  2.7 3.0 %collective-permute-start = (bf16[4,128]{1,0:T(4,128)(2,1)S(1)}, bf16[4,128]{1,0:T(4,128)(2,1)S(1)}, u32[]{:S(2)}, u32[]{:S(2)}) collective-permute-start(bf16[4,128]{1,0:T(4,128)(2,1)S(1)} %get-tuple-element.7), channel_id=1, source_target_pairs={{0,4},{4,0},{8,12},{12,8},{16,20},{20,16},{24,28},{28,24},{1,5},{5... | collective-permute-start | bytes 3080 | tf_op jit(solution)/shard_map/ppermute | solution.py:28
  5.8 1.4 reshape.95
  7.2 0.0 copy-done.2
  7.2 0.1 convert_multiply_fusion.4
  7.3 0.2 mul.133
  7.5 0.0 copy-done.3
  7.5 0.2 reshape.100
  7.7 0.1 copy.75
  7.9 0.9 copy.76
  8.7 1.4 exponential_multiply_fusion
  10.1 1.0 fusion.39
  11.1 0.0 copy-done
  11.1 6.1 %convolution_bitcast_fusion = f32[5,4,128,256]{3,0,2,1:T(8,128)S(1)} fusion(f32[4,4,128,256]{3,2,1,0:T(8,128)S(1)} %fusion.39, f32[4,4,128]{0,2,1:T(8,128)S(1)} %copy-done, f32[5,4,128]{0,2,1:T(8,128)S(1)} %copy.75, pred[5,4]{0,1:T(4,128)(4,1)S(1)} %iota_compare_fusion.2), kind=kOutput, calls=%fused_computation.8 | convolution fusion | flops 31477760 | bytes 4737044 | tf_op jit(solution)/shard_map/nmhd,mhdv->nhdv/dot_general | solution.py:867
  17.2 0.5 slice.26
  17.8 0.7 copy.120
  18.5 0.0 collective-permute-start.2
  18.6 0.4 slice.25
  18.9 0.0 copy-start.8
  18.9 1.8 fusion.16
  20.7 1.8 convolution_select_fusion
  22.5 0.0 collective-permute-done
  22.5 2.1 %collective-permute-start.1 = (bf16[4,128]{1,0:T(4,128)(2,1)S(1)}, bf16[4,128]{1,0:T(4,128)(2,1)S(1)}, u32[]{:S(2)}, u32[]{:S(2)}) collective-permute-start(bf16[4,128]{1,0:T(4,128)(2,1)S(1)} %get-tuple-element.5), channel_id=1, source_target_pairs={{0,8},{4,12},{8,0},{12,4},{16,24},{20,28},{24,16},{28,20},{1,9},{5... | collective-permute-start | bytes 3080 | tf_op jit(solution)/shard_map/ppermute | solution.py:28
  24.6 1.9 %collective-permute-done.2 = bf16[4,128,256]{2,1,0:T(8,128)(2,1)S(1)} collective-permute-done((bf16[4,128,256]{2,1,0:T(8,128)(2,1)}, bf16[4,128,256]{2,1,0:T(8,128)(2,1)S(1)}, u32[]{:S(2)}, u32[]{:S(2)}) %collective-permute-start.2) | collective-permute-done | bytes 262176 | tf_op jit(solution)/shard_map/ppermute | solution.py:28
  26.5 0.9 fusion.61
  27.4 1.6 collective-permute-start.3
  29.0 1.6 fusion.20
  30.6 0.0 copy-done.8
  30.6 0.0 collective-permute-done.1
  30.7 4.0 %collective-permute-done.3 = bf16[4,128,256]{2,1,0:T(8,128)(2,1)} collective-permute-done((bf16[4,128,256]{2,1,0:T(8,128)(2,1)}, bf16[4,128,256]{2,1,0:T(8,128)(2,1)}, u32[]{:S(2)}, u32[]{:S(2)}) %collective-permute-start.3) | collective-permute-done | bytes 262176 | tf_op jit(solution)/shard_map/ppermute | solution.py:28
  34.6 1.3 fusion.33
  35.9 4.5 %collective-permute-start.4 = (bf16[4,128,256]{2,1,0:T(8,128)(2,1)S(1)}, bf16[4,128,256]{2,1,0:T(8,128)(2,1)S(1)}, u32[]{:S(2)}, u32[]{:S(2)}) collective-permute-start(bf16[4,128,256]{2,1,0:T(8,128)(2,1)S(1)} %fusion.33), channel_id=1, source_target_pairs={{0,16},{4,20},{8,24},{12,28},{1,17},{5,21},{9,25},{13,29},{2,18},{... | collective-permute-start | bytes 786440 | tf_op jit(solution)/shard_map/ppermute | solution.py:28
  40.5 3.8 %collective-permute-done.4 = bf16[4,128,256]{2,1,0:T(8,128)(2,1)S(1)} collective-permute-done((bf16[4,128,256]{2,1,0:T(8,128)(2,1)S(1)}, bf16[4,128,256]{2,1,0:T(8,128)(2,1)S(1)}, u32[]{:S(2)}, u32[]{:S(2)}) %collective-permute-start.4) | collective-permute-done | bytes 262176 | tf_op jit(solution)/shard_map/ppermute | solution.py:28
  44.3 2.4 %multiply_reduce_fusion = (f32[4,64,4]{1,2,0:T(4,128)S(1)}, f32[4,64,4,256]{3,1,2,0:T(8,128)S(1)}) fusion(f32[4,64,4,256]{3,1,2,0:T(8,128)S(1)} %fusion.20, f32[4,64,4,128]{3,2,1,0:T(4,128)} %get-tuple-element.15, bf16[4,128,256]{2,1,0:T(8,128)(2,1)S(1)} %collective-permute-done.2, bf16[4,128,256]{2,1,0:T(8,128)(2,1)} %collective-permute-done.3, ...), kind=kOutput, calls=%fused_computation.31 | convolution fusion | flops 404749312 | bytes 3416067 | tf_op jit(solution)/shard_map/nthd,hdv->nthv/dot_general | solution.py:904
  46.8 0.0 copy-start.1
  46.8 0.1 copy.85
  46.9 0.3 mul.153
  47.2 0.2 copy.90
  47.5 0.7 copy.81
  48.1 0.0 copy-start.5
  48.1 0.0 copy-start.4
  48.2 0.0 copy-start.6
  48.2 0.2 copy.89
  48.4 0.0 copy-done.1
  48.4 0.4 fusion.28
  48.8 1.6 collective-permute-start.5
  50.4 9.3 %collective-permute-done.5 = bf16[256,1024]{1,0:T(8,128)(2,1)S(1)} collective-permute-done((bf16[256,1024]{1,0:T(8,128)(2,1)S(1)}, bf16[256,1024]{1,0:T(8,128)(2,1)S(1)}, u32[]{:S(2)}, u32[]{:S(2)}) %collective-permute-start.5) | collective-permute-done | bytes 524320 | tf_op jit(solution)/shard_map/ppermute | solution.py:28
  59.7 0.1 pad_maximum_fusion
  59.8 0.1 collective-permute-start.6
  59.9 0.0 copy-done.5
  59.9 0.6 reshape.102.gain_ref
  60.5 0.0 copy-done.4
  60.5 0.0 copy-done.6
  60.6 0.6 select_reduce_fusion.table_ref
  61.2 2.5 %constant_dynamic-slice_fusion.3 = (bf16[1024,512]{1,0:T(8,128)(2,1)S(1)}, bf16[1024,512]{1,0:T(8,128)(2,1)S(1)}, bf16[1024,512]{1,0:T(8,128)(2,1)S(1)}, bf16[1024,512]{1,0:T(8,128)(2,1)S(1)}) fusion(bf16[4096,512]{1,0:T(8,128)(2,1)} %param.25, s32[]{:T(128)S(6)} %select_n.108, s32[]{:T(128)S(6)} %select_n.109, s32[]{:T(128)S(6)} %select_n.111, ...), kind=kLoop, calls=%fused_computation.104 | loop fusion | bytes 8388624 | tf_op jit(solution)/shard_map/dynamic_slice | solution.py:65
  63.7 0.0 collective-permute-done.6
  63.7 0.0 copy-done.7
  63.7 2.0 %add_convert_fusion.mid_ref = bf16[256,512]{1,0:T(8,128)(2,1)} fusion(bf16[256,512]{1,0:T(8,128)(2,1)S(1)} %copy-done.7, bf16[1024,512]{1,0:T(8,128)(2,1)S(1)} %get-tuple-element.13, bf16[1024,512]{1,0:T(8,128)(2,1)S(1)} %get-tuple-element.14, bf16[1024,512]{1,0:T(8,128)(2,1)S(1)} %get-tuple-element.12, bf16[1024,512]{1,0:T(8,128)(2,1)S(1)} %get-tuple-element.11, ...), kind=kOutput, calls=%fused_computation.58 | convolution fusion | flops 1097203712 | bytes 6815744 | tf_op jit(solution)/shard_map/dot_general | solution.py:920
  65.7 115.8 %exchange_experts.1 = bf16[256,512]{1,0:T(8,128)(2,1)} custom-call(bf16[256,512]{1,0:T(8,128)(2,1)} %add_convert_fusion.mid_ref, f32[8,256]{1,0:T(8,128)} %reshape.102.gain_ref, f32[8,256]{1,0:T(8,128)} %select_reduce_fusion.table_ref, bf16[2048,256]{1,0:T(8,128)(2,1)} %gate_hbm.1, bf16[2048,256]{1,0:T(8,128)(2,1)} %up_hbm.1, bf16[256,2048]{1,0:T(8,128)(2,1)} %down_hbm.1, ...), custom_call_target="tpu_custom_call" | custom-call | tf_op jit(solution)/shard_map/exchange_experts/pallas_call | solution.py:756
  181.5 1.7 copy.122
  (21 shorter events, 0.1 us)
Async XLA Ops:
  0.0 7.2 %copy-start.2 = (bf16[256,512]{1,0:T(8,128)(2,1)S(1)}, bf16[256,512]{1,0:T(8,128)(2,1)}, u32[]{:S(2)}) copy-start(bf16[256,512]{1,0:T(8,128)(2,1)} %param.18) | copy-start | bytes 786436
  0.0 7.5 %copy-start.3 = (bf16[256,512]{1,0:T(8,128)(2,1)S(1)}, bf16[256,512]{1,0:T(8,128)(2,1)}, u32[]{:S(2)}) copy-start(bf16[256,512]{1,0:T(8,128)(2,1)} %param.19) | copy-start | bytes 786436
  2.7 19.7 %collective-permute-start = (bf16[4,128]{1,0:T(4,128)(2,1)S(1)}, bf16[4,128]{1,0:T(4,128)(2,1)S(1)}, u32[]{:S(2)}, u32[]{:S(2)}) collective-permute-start(bf16[4,128]{1,0:T(4,128)(2,1)S(1)} %get-tuple-element.7), channel_id=1, source_target_pairs={{0,4},{4,0},{8,12},{12,8},{16,20},{20,16},{24,28},{28,24},{1,5},{5... | collective-permute-start | bytes 3080 | tf_op jit(solution)/shard_map/ppermute | solution.py:28
  8.7 2.4 %copy-start = (f32[4,4,128]{0,2,1:T(8,128)S(1)}, f32[4,4,128]{0,2,1:T(8,128)}, u32[]{:S(2)}) copy-start(f32[4,4,128]{0,2,1:T(8,128)} %copy.76) | copy-start | bytes 24580
  18.5 8.0 %collective-permute-start.2 = (bf16[4,128,256]{2,1,0:T(8,128)(2,1)}, bf16[4,128,256]{2,1,0:T(8,128)(2,1)S(1)}, u32[]{:S(2)}, u32[]{:S(2)}) collective-permute-start(bf16[4,128,256]{2,1,0:T(8,128)(2,1)} %bitcast.70), channel_id=1, source_target_pairs={{0,4},{4,0},{8,12},{12,8},{16,20},{20,16},{24,28},{28,24},{1,5},{5... | collective-permute-start | bytes 786440 | tf_op jit(solution)/shard_map/ppermute | solution.py:28
  18.9 11.7 %copy-start.8 = (bf16[256]{0:T(256)(128)(2,1)S(1)}, bf16[256]{0:T(256)(128)(2,1)}, u32[]{:S(2)}) copy-start(bf16[256]{0:T(256)(128)(2,1)} %param.24) | copy-start | bytes 1540
  22.5 8.2 %collective-permute-start.1 = (bf16[4,128]{1,0:T(4,128)(2,1)S(1)}, bf16[4,128]{1,0:T(4,128)(2,1)S(1)}, u32[]{:S(2)}, u32[]{:S(2)}) collective-permute-start(bf16[4,128]{1,0:T(4,128)(2,1)S(1)} %get-tuple-element.5), channel_id=1, source_target_pairs={{0,8},{4,12},{8,0},{12,4},{16,24},{20,28},{24,16},{28,20},{1,9},{5... | collective-permute-start | bytes 3080 | tf_op jit(solution)/shard_map/ppermute | solution.py:28
  27.4 7.2 %collective-permute-start.3 = (bf16[4,128,256]{2,1,0:T(8,128)(2,1)}, bf16[4,128,256]{2,1,0:T(8,128)(2,1)}, u32[]{:S(2)}, u32[]{:S(2)}) collective-permute-start(bf16[4,128,256]{2,1,0:T(8,128)(2,1)} %fusion.61), channel_id=1, source_target_pairs={{0,8},{4,12},{8,0},{12,4},{16,24},{20,28},{24,16},{28,20},{1,9},{5... | collective-permute-start | bytes 786440 | tf_op jit(solution)/shard_map/ppermute | solution.py:28
  35.9 8.4 %collective-permute-start.4 = (bf16[4,128,256]{2,1,0:T(8,128)(2,1)S(1)}, bf16[4,128,256]{2,1,0:T(8,128)(2,1)S(1)}, u32[]{:S(2)}, u32[]{:S(2)}) collective-permute-start(bf16[4,128,256]{2,1,0:T(8,128)(2,1)S(1)} %fusion.33), channel_id=1, source_target_pairs={{0,16},{4,20},{8,24},{12,28},{1,17},{5,21},{9,25},{13,29},{2,18},{... | collective-permute-start | bytes 786440 | tf_op jit(solution)/shard_map/ppermute | solution.py:28
  46.8 1.6 copy-start.1
  48.1 11.8 %copy-start.5 = (bf16[2048]{0:T(1024)(128)(2,1)S(1)}, bf16[2048]{0:T(1024)(128)(2,1)}, u32[]{:S(2)}) copy-start(bf16[2048]{0:T(1024)(128)(2,1)} %param.27) | copy-start | bytes 12292
  48.1 12.4 %copy-start.4 = (f32[256,4]{0,1:T(4,128)S(1)}, f32[256,4]{0,1:T(4,128)}, u32[]{:S(2)}) copy-start(f32[256,4]{0,1:T(4,128)} %param.29) | copy-start | bytes 12292
  48.2 12.4 %copy-start.6 = (s32[256,4]{0,1:T(4,128)S(1)}, s32[256,4]{0,1:T(4,128)}, u32[]{:S(2)}) copy-start(s32[256,4]{0,1:T(4,128)} %param.28) | copy-start | bytes 12292
  48.8 10.9 %collective-permute-start.5 = (bf16[256,1024]{1,0:T(8,128)(2,1)S(1)}, bf16[256,1024]{1,0:T(8,128)(2,1)S(1)}, u32[]{:S(2)}, u32[]{:S(2)}) collective-permute-start(bf16[256,1024]{1,0:T(8,128)(2,1)S(1)} %fusion.28), channel_id=1, source_target_pairs={{0,2},{1,3},{2,0},{3,1},{4,6},{5,7},{6,4},{7,5},{8,10},{9,11},{10,... | collective-permute-start | bytes 1572872 | tf_op jit(solution)/shard_map/ppermute | solution.py:28
  59.8 3.9 %collective-permute-start.6 = (bf16[256,2048]{1,0:T(8,128)(2,1)S(1)}, bf16[256,2048]{1,0:T(8,128)(2,1)S(1)}, u32[]{:S(2)}, u32[]{:S(2)}) collective-permute-start(bf16[256,2048]{1,0:T(8,128)(2,1)S(1)} %pad_maximum_fusion), channel_id=1, source_target_pairs={{0,1},{1,0},{2,3},{3,2},{4,5},{5,4},{6,7},{7,6},{8,9},{9,8},{10,11... | collective-permute-start | bytes 3145736 | tf_op jit(solution)/shard_map/ppermute | solution.py:28
  61.2 2.5 %copy-start.7 = (bf16[256,512]{1,0:T(8,128)(2,1)S(1)}, bf16[256,512]{1,0:T(8,128)(2,1)}, u32[]{:S(2)}) copy-start(bf16[256,512]{1,0:T(8,128)(2,1)} %param.26) | copy-start | bytes 786436

commit v2 on v1

--- a/solution.py
+++ b/solution.py
@@ -11,8 +11,6 @@
 DV = 256
 BLOCK_POSITIONS = 64
 FF_PARTS = 4
-CHUNKS = 4
-
 
 HIGHEST = lax.Precision.HIGHEST
 EPSILON = 1e-06
@@ -97,92 +95,6 @@
     return value
 
 
-def dot_halves(halves, matrix):
-    parts = jnp.split(matrix, 2, 0)
-    return sum(
-        jnp.dot(half, part, preferred_element_type=jnp.float32)
-        for half, part in zip(halves, parts)
-    )
-
-
-def dense_experts(
-    mid_local,
-    feedforward_gain,
-    routing,
-    router_score,
-    expert_gate_weight,
-    expert_up_weight,
-    expert_down_weight,
-    shared_expert_gate,
-    shared_expert_up,
-    shared_expert_down,
-):
-    tokens = mid_local.shape[0]
-    hidden_width = expert_gate_weight.shape[1]
-    sp_index, tp_index = lax.axis_index("sp"), lax.axis_index("tp")
-    sp_steps = [("sp", bit) for bit in range(lax.axis_size("sp").bit_length() - 1)][::-1]
-    tp_steps = [("tp", bit) for bit in range(lax.axis_size("tp").bit_length() - 1)][::-1]
-    plans = (
-        sp_steps + tp_steps,
-        sp_steps[:-1] + tp_steps[:-1] + sp_steps[-1:] + tp_steps[-1:],
-    )
-    column_masks = masks_of(tp_steps, "tp")
-    slab = mid_local.shape[1]
-    gain = lax.dynamic_slice_in_dim(feedforward_gain, tp_index * slab, slab, 0)
-    mid_float = mid_local.astype(jnp.float32)
-    scaled = (mid_float * gain.astype(jnp.float32)).astype(jnp.bfloat16)
-    squares = jnp.sum(mid_float * mid_float, axis=-1)
-    for axis, bit in tp_steps:
-        squares = squares + from_partner(squares, axis, bit)
-    inverse_own = lax.rsqrt(squares / (slab * lax.axis_size("tp")) + EPSILON)
-    inverse_here = spread(inverse_own[None], sp_steps)
-    gate = relative_rows(expert_gate_weight, tp_index, column_masks)
-    up = relative_rows(expert_up_weight, tp_index, column_masks)
-    down = relative_columns(expert_down_weight, tp_index, column_masks)
-    shared_gate = relative_rows(shared_expert_gate, tp_index, column_masks)
-    shared_up = relative_rows(shared_expert_up, tp_index, column_masks)
-    shared_down = relative_rows(shared_expert_down, tp_index, column_masks)
-    route_weight = ROUTE_SCALE * router_score / jnp.sum(router_score, axis=1, keepdims=True)
-    expert_ids = jnp.arange(lax.axis_size("sp"), dtype=jnp.int32)
-    weight_table = jnp.sum(
-        jnp.where(routing[:, :, None] == expert_ids, route_weight[:, :, None], 0.0), axis=1
-    )
-    weight_all = spread(weight_table.T[None], sp_steps)
-    weight_here = lax.dynamic_index_in_dim(weight_all, sp_index, 1, False)
-    rows = tokens // CHUNKS
-    own_halves, routed = [], []
-    for chunk in range(CHUNKS):
-        steps = plans[chunk % 2]
-        axis, bit = steps[-1]
-        span = slice(chunk * rows, (chunk + 1) * rows)
-        near = spread(scaled[span], steps[:-1])
-        halves = (near, from_partner(near, axis, bit))
-        own_halves.append([half[:rows] for half in halves])
-        row_inverse = inverse_here[:, span].reshape(-1, 1)
-        row_weight = weight_here[:, span].reshape(-1, 1)
-        hidden = (
-            jax.nn.silu(dot_halves(halves, gate) * row_inverse)
-            * (dot_halves(halves, up) * row_inverse)
-            * row_weight
-        ).astype(jnp.bfloat16)
-        kept_down, given_down = jnp.split(down, 2, 1)
-        given = jnp.dot(hidden, given_down, preferred_element_type=jnp.float32).astype(jnp.bfloat16)
-        kept = jnp.dot(hidden, kept_down, preferred_element_type=jnp.float32)
-        summed = (kept + from_partner(given, axis, bit).astype(jnp.float32)).astype(jnp.bfloat16)
-        routed.append(collect(summed, steps[:-1]))
-    own_halves = [jnp.concatenate(parts, 0) for parts in zip(*own_halves)]
-    shared_hidden = (
-        jax.nn.silu(dot_halves(own_halves, shared_gate) * inverse_own[:, None])
-        * (dot_halves(own_halves, shared_up) * inverse_own[:, None])
-    ).astype(jnp.bfloat16)
-    shared_out = jnp.dot(
-        spread(shared_hidden, tp_steps), shared_down, preferred_element_type=jnp.float32
-    )
-    routed = jnp.concatenate(routed, 0).astype(jnp.float32)
-    return (mid_float + routed + shared_out).astype(jnp.bfloat16)
-
-
-SLAB_HALF = 256
 EXPERT_PARTS = 3
 
 
@@ -205,7 +117,8 @@
     most,
     mid_ref,
     gain_ref,
-    table_ref,
+    routing_ref,
+    score_ref,
     gate_hbm,
     up_hbm,
     down_hbm,
@@ -219,6 +132,7 @@
     shared_gate_ref,
     shared_up_ref,
     shared_down_ref,
+    table_ref,
     tables,
     ranks,
     slot_weights,
@@ -336,6 +250,17 @@
     ]
     for load in loads:
         load.start()
+    score = score_ref[...]
+    route_weight = ROUTE_SCALE * score / jnp.sum(score, axis=0, keepdims=True)
+    experts_here = lax.broadcasted_iota(jnp.int32, table_ref.shape, 0)
+    table = jnp.zeros(table_ref.shape, f32)
+    for pick_at in range(score.shape[0]):
+        table = table + jnp.where(
+            routing_ref[pick_at : pick_at + 1, :] == experts_here,
+            route_weight[pick_at : pick_at + 1, :],
+            0.0,
+        )
+    table_ref[...] = table
     pl.semaphore_wait(barrier, len(peers))
 
     low, high = mid_ref.at[:, pl.ds(0, half)], mid_ref.at[:, pl.ds(half, half)]
@@ -486,7 +411,7 @@
             pieces, squares = [], None
             for number in range(parts):
                 rows = expert_rows[number, source]
-                pieces.append(rows * gain_ref[pl.ds(number, 1), :].astype(bf16))
+                pieces.append(rows * gain_ref[:, number * half : (number + 1) * half])
                 wide = rows.astype(f32)
                 squares = wide * wide if squares is None else squares + wide * wide
             inverse = lax.rsqrt(jnp.sum(squares, axis=1, keepdims=True) / width + EPSILON)
@@ -633,8 +558,8 @@
         for rows, number in blocks:
             wide = rows.astype(f32)
             squares = squares + wide * wide
-            scaled = rows * gain_ref[pl.ds(number, 1), :].astype(bf16)
             span = pl.ds(pl.multiple_of(number * half, half), half)
+            scaled = rows * gain_ref[:, span]
             gate = gate + jnp.dot(scaled, shared_gate_ref[span, :], preferred_element_type=f32)
             up = up + jnp.dot(scaled, shared_up_ref[span, :], preferred_element_type=f32)
         inverse = lax.rsqrt(jnp.sum(squares, axis=1, keepdims=True) / width + EPSILON)
@@ -730,15 +655,7 @@
     parts = 2 * tp_count
     picked = routing.shape[1]
     most = 3 * tokens * picked // (2 * sp_count)
-    route_weight = ROUTE_SCALE * router_score / jnp.sum(router_score, axis=1, keepdims=True)
-    expert_ids = jnp.arange(sp_count, dtype=jnp.int32)
-    table = jnp.sum(
-        jnp.where(
-            routing.T[None, :, :] == expert_ids[:, None, None], route_weight.T[None, :, :], 0.0
-        ),
-        axis=1,
-    )
-    gain = feedforward_gain.astype(jnp.float32).reshape(parts, half)
+    gain = feedforward_gain.reshape(1, parts * half)
     bf16, f32 = jnp.bfloat16, jnp.float32
     vmem = pltpu.VMEM
     dma = pltpu.SemaphoreType.DMA
@@ -757,10 +674,11 @@
         functools.partial(exchange_kernel, most),
         name="exchange_experts",
         out_shape=jax.ShapeDtypeStruct(mid_local.shape, bf16),
-        in_specs=[in_vmem] * 3 + [in_any] * len(weights),
+        in_specs=[in_vmem] * 4 + [in_any] * len(weights),
         out_specs=in_vmem,
         scratch_shapes=[vmem(weight.shape, bf16) for weight in weights]
         + [
+            vmem((sp_count, tokens), f32),
             vmem((sp_count, sp_count, tokens), f32),
             vmem((sp_count, sp_count, tokens), f32),
             vmem((sp_count, most, 128), f32),
@@ -820,7 +738,353 @@
         compiler_params=pltpu.CompilerParams(
             collective_id=1, has_side_effects=True, vmem_limit_bytes=60 * 1024 * 1024
         ),
-    )(mid_local, gain, table, *weights)
+    )(mid_local, gain, routing.T, router_score.T, *weights)
+
+
+def attend_kernel(
+    extra_ref,
+    norm_gain_ref,
+    decay_hbm,
+    key_hbm,
+    value_hbm,
+    query_hbm,
+    gate_hbm,
+    residual_hbm,
+    projection_hbm,
+    out_ref,
+    decay_ref,
+    key_ref,
+    value_ref,
+    query_ref,
+    gate_ref,
+    residual_ref,
+    projection_ref,
+    inside,
+    query_start,
+    decays,
+    decays_in,
+    state_out,
+    state_in,
+    carry_out,
+    carry_in,
+    local_mixed,
+    head_rows,
+    total,
+    load_sem,
+    decay_sems,
+    state_send,
+    state_recv,
+    carry_send,
+    carry_recv,
+    y_send,
+    y_recv,
+    core_send,
+    core_recv,
+    pass_send,
+    pass_recv,
+):
+    bf16, f32 = jnp.bfloat16, jnp.float32
+    sp_count, tp_count = lax.axis_size("sp"), lax.axis_size("tp")
+    depth = sp_count // 2
+    head_count, tokens = extra_ref.shape
+    blocks = tokens // BLOCK_POSITIONS
+    sp, tp = lax.axis_index("sp"), lax.axis_index("tp")
+    z, x = sp // 2, sp % 2
+    y, core = tp // 2, tp % 2
+    tp_y = (1 - y) * 2 + core
+    tp_core = y * 2 + (1 - core)
+    tp_far = (1 - y) * 2 + (1 - core)
+    side, right = (z * 2 + 1 - x, tp), (sp + 2, tp)
+    over_y, over_core = (sp, tp_y), (sp, tp_core)
+    has_left, has_right = z > 0, z < depth - 1
+    pending = []
+
+    def begin(copy, when=None):
+        if when is None:
+            copy.start()
+        else:
+            pl.when(when)(copy.start)
+        pending.append((copy, when))
+
+    def arrive(target, sem):
+        remote(target, target, decay_sems.at[0], sem, (sp, tp)).wait_recv()
+
+    arrays = [
+        (decay_hbm, decay_ref),
+        (key_hbm, key_ref),
+        (value_hbm, value_ref),
+        (query_hbm, query_ref),
+        (gate_hbm, gate_ref),
+        (residual_hbm, residual_ref),
+        (projection_hbm, projection_ref),
+    ]
+    loads = [
+        pltpu.make_async_copy(hbm, ref, load_sem.at[number])
+        for number, (hbm, ref) in enumerate(arrays)
+    ]
+    for load in loads:
+        load.start()
+    barrier = pltpu.get_barrier_semaphore()
+    for peer in (side, over_y, over_core):
+        pl.semaphore_signal(barrier, inc=1, device_id=peer, device_id_type=pl.DeviceIdType.MESH)
+    for peer, exists in (((sp - 2, tp), has_left), (right, has_right)):
+        @pl.when(exists)
+        def _():
+            pl.semaphore_signal(
+                barrier, inc=1, device_id=peer, device_id_type=pl.DeviceIdType.MESH
+            )
+
+    row = lax.broadcasted_iota(jnp.int32, (tokens, tokens), 0)
+    column = lax.broadcasted_iota(jnp.int32, (tokens, tokens), 1)
+    causal = jnp.logical_and(
+        column <= row, row // BLOCK_POSITIONS == column // BLOCK_POSITIONS
+    )
+    triangle = jnp.where(causal, 1.0, 0.0).astype(f32)
+    over_first, over_rows = (((0,), (0,)), ((), ())), (((1,), (1,)), ((), ()))
+    owner = (
+        lax.broadcasted_iota(jnp.int32, (head_count, head_count * DK), 1) // DK
+        == lax.broadcasted_iota(jnp.int32, (head_count, head_count * DK), 0)
+    )
+    extra = lax.dot_general(
+        extra_ref[...],
+        jnp.where(owner, 1.0, 0.0),
+        over_first,
+        precision=HIGHEST,
+        preferred_element_type=f32,
+    )
+    loads[0].wait()
+    preactivation = decay_ref[...].astype(f32)
+    logs = jnp.minimum(preactivation, 0.0) - jnp.log1p(jnp.exp(-jnp.abs(preactivation)))
+    logs = logs / GATE_TEMPER + extra
+    inside[...] = jnp.dot(triangle, logs, precision=HIGHEST, preferred_element_type=f32)
+    ends = [
+        inside[(block + 1) * BLOCK_POSITIONS - 1 : (block + 1) * BLOCK_POSITIONS, :]
+        for block in range(blocks)
+    ]
+    before = [jnp.zeros_like(ends[0])]
+    for end in ends:
+        before.append(before[-1] + end)
+    decays[...] = jnp.broadcast_to(jnp.exp(before[blocks]), decays.shape)
+
+    def span(block):
+        return slice(block * BLOCK_POSITIONS, (block + 1) * BLOCK_POSITIONS)
+
+    def columns(head, width):
+        return slice(head * width, (head + 1) * width)
+
+    loads[1].wait()
+    loads[2].wait()
+    pl.semaphore_wait(
+        barrier, 3 + jnp.where(has_left, 1, 0) + jnp.where(has_right, 1, 0)
+    )
+    begin(remote(decays, decays_in, decay_sems.at[1], decay_sems.at[2], side))
+    for head in range(head_count):
+        wide = columns(head, DK)
+        tail = jnp.concatenate(
+            [
+                before[blocks][:, wide] - before[block][:, wide] - inside[span(block), wide]
+                for block in range(blocks)
+            ],
+            axis=0,
+        )
+        faded = (key_ref[:, wide].astype(f32) * jnp.exp(tail)).astype(bf16)
+        state_out[head] = lax.dot_general(
+            value_ref[:, columns(head, DV)], faded, over_first, preferred_element_type=f32
+        ).astype(bf16)
+        begin(
+            remote(
+                state_out.at[head],
+                state_in.at[head],
+                state_send.at[head],
+                state_recv.at[head],
+                side,
+            )
+        )
+
+    def local(head):
+        wide = columns(head, DK)
+        values = value_ref[:, columns(head, DV)]
+        keys = key_ref[:, wide].astype(f32)
+        logs_inside = inside[:, wide]
+        queries = query_ref[:, wide].astype(f32) * (DK**-0.5) * jnp.exp(logs_inside)
+        query_decay = queries.astype(bf16)
+        key_decay = (keys * jnp.exp(-logs_inside)).astype(bf16)
+        scores = lax.dot_general(
+            query_decay, key_decay, over_rows, preferred_element_type=f32
+        )
+        scores = jnp.where(causal, scores, 0.0).astype(bf16)
+        mixed = jnp.dot(scores, values, preferred_element_type=f32)
+        state, pieces, starts = None, [mixed[span(0)]], []
+        for block in range(blocks):
+            starts.append(queries[span(block)] * jnp.exp(before[block][:, wide]))
+            if block == blocks - 1:
+                break
+            end = ends[block][:, wide]
+            key_end = (keys[span(block)] * jnp.exp(end - logs_inside[span(block)])).astype(bf16)
+            fresh = lax.dot_general(
+                values[span(block)], key_end, over_first, preferred_element_type=f32
+            )
+            state = fresh if state is None else state * jnp.exp(end) + fresh
+            passed = lax.dot_general(
+                query_decay[span(block + 1)],
+                state.astype(bf16),
+                over_rows,
+                preferred_element_type=f32,
+            )
+            pieces.append(mixed[span(block + 1)] + passed)
+        local_mixed[head] = jnp.concatenate(pieces, axis=0)
+        query_start[head] = jnp.concatenate(starts, axis=0).astype(bf16)
+
+    def chain(head):
+        wide = columns(head, DK)
+        arrive(state_in.at[head], state_recv.at[head])
+        own, other = state_out[head].astype(f32), state_in[head].astype(f32)
+        decay_own, decay_other = decays[0:1, wide], decays_in[0:1, wide]
+        first = jnp.where(x == 0, own, other)
+        second = jnp.where(x == 0, other, own)
+        decay_second = jnp.where(x == 0, decay_other, decay_own)
+
+        @pl.when(has_left)
+        def _():
+            arrive(carry_in.at[head], carry_recv.at[head])
+
+        entering = jnp.where(has_left, carry_in[head].astype(f32), 0.0)
+        carry_out[head] = (
+            decay_own * decay_other * entering + decay_second * first + second
+        ).astype(bf16)
+        begin(
+            remote(
+                carry_out.at[head],
+                carry_in.at[head],
+                carry_send.at[head],
+                carry_recv.at[head],
+                right,
+            ),
+            has_right,
+        )
+        return jnp.where(x == 0, entering, decay_other * entering + other).astype(bf16)
+
+    def finish(head, entering):
+        mixed = local_mixed[head] + lax.dot_general(
+            query_start[head], entering, over_rows, preferred_element_type=f32
+        )
+        inverse = lax.rsqrt(jnp.mean(mixed * mixed, axis=1, keepdims=True) + EPSILON)
+        opened = swish(gate_ref[:, columns(head, DV)].astype(f32))
+        head_rows[tp, head] = (
+            mixed * inverse * norm_gain_ref[...].astype(f32) * opened
+        ).astype(bf16)
+        source = head_rows.at[tp, head]
+        begin(remote(source, source, y_send.at[head], y_recv.at[head], over_y))
+        begin(remote(source, source, core_send.at[head], core_recv.at[head], over_core))
+
+    def project(owner, head):
+        start = (owner * head_count + head) * DV
+        return jnp.dot(
+            head_rows[owner, head],
+            projection_ref[pl.ds(pl.multiple_of(start, DV), DV), :],
+            preferred_element_type=f32,
+        )
+
+    def relay(head):
+        target = head_rows.at[tp_y, head]
+        arrive(target, y_recv.at[head])
+        begin(remote(target, target, pass_send.at[head], pass_recv.at[head], over_core))
+
+    loads[3].wait()
+    for head in range(head_count):
+        local(head)
+    loads[4].wait()
+    arrive(decays_in, decay_sems.at[2])
+    for head in range(head_count):
+        entering = chain(head)
+        finish(head, entering)
+        if head >= 2:
+            relay(head - 2)
+    loads[5].wait()
+    loads[6].wait()
+    total[...] = residual_ref[...].astype(f32) + sum(
+        project(tp, head) for head in range(head_count)
+    )
+    for head in range(head_count):
+        arrive(head_rows.at[tp_core, head], core_recv.at[head])
+    total[...] = total[...] + sum(project(tp_core, head) for head in range(head_count))
+    for head in range(head_count):
+        if head >= 2:
+            relay(head)
+    for head in range(head_count):
+        total[...] = total[...] + project(tp_y, head)
+        arrive(head_rows.at[tp_far, head], pass_recv.at[head])
+        total[...] = total[...] + project(tp_far, head)
+    out_ref[...] = total[...].astype(bf16)
+    for copy, when in pending:
+        if when is None:
+            copy.wait_send()
+        else:
+            pl.when(when)(copy.wait_send)
+
+
+def attend_project(
+    queries,
+    key_matrix,
+    value_matrix,
+    output_gate_preactivation,
+    decay_preactivation,
+    extra_log_decay,
+    head_norm_gain,
+    residual,
+    output_projection,
+):
+    bf16, f32 = jnp.bfloat16, jnp.float32
+    arrays = (
+        decay_preactivation,
+        key_matrix,
+        value_matrix,
+        queries,
+        output_gate_preactivation,
+        residual,
+        output_projection,
+    )
+    tokens, head_count = extra_log_decay.shape
+    tp_count = lax.axis_size("tp")
+    vmem, dma = pltpu.VMEM, pltpu.SemaphoreType.DMA
+    in_vmem = pl.BlockSpec(memory_space=pltpu.VMEM)
+    in_any = pl.BlockSpec(memory_space=pl.ANY)
+    return pl.pallas_call(
+        attend_kernel,
+        name="attend_project",
+        out_shape=jax.ShapeDtypeStruct(residual.shape, bf16),
+        in_specs=[in_vmem] * 2 + [in_any] * len(arrays),
+        out_specs=in_vmem,
+        scratch_shapes=[vmem(array.shape, bf16) for array in arrays]
+        + [
+            vmem((tokens, head_count * DK), f32),
+            vmem((head_count, tokens, DK), bf16),
+            vmem((8, head_count * DK), f32),
+            vmem((8, head_count * DK), f32),
+            vmem((head_count, DV, DK), bf16),
+            vmem((head_count, DV, DK), bf16),
+            vmem((head_count, DV, DK), bf16),
+            vmem((head_count, DV, DK), bf16),
+            vmem((head_count, tokens, DV), f32),
+            vmem((tp_count, head_count, tokens, DV), bf16),
+            vmem(residual.shape, f32),
+            dma((len(arrays),)),
+            dma((3,)),
+            dma((head_count,)),
+            dma((head_count,)),
+            dma((head_count,)),
+            dma((head_count,)),
+            dma((head_count,)),
+            dma((head_count,)),
+            dma((head_count,)),
+            dma((head_count,)),
+            dma((head_count,)),
+            dma((head_count,)),
+        ],
+        compiler_params=pltpu.CompilerParams(
+            collective_id=2, has_side_effects=True, vmem_limit_bytes=62 * 1024 * 1024
+        ),
+    )(extra_log_decay.T, head_norm_gain.reshape(1, DV), *arrays)
 
 
 def attention_heads(queries, key_matrix, value_matrix, decay_preactivation, extra_log_decay):
@@ -892,39 +1156,18 @@
 ):
     tokens = queries.shape[0]
     local_head_count = extra_log_decay.shape[1]
-    local_part, query_start, dev_decay, dev_update = attention_heads(
-        queries, key_matrix, value_matrix, decay_preactivation, extra_log_decay
-    )
-    _, entering = prefix(
-        (dev_decay, dev_update),
-        "sp",
-        carry_combine,
-        (jnp.ones_like(dev_decay), jnp.zeros_like(dev_update)),
-    )
-    attention_output = local_part + jnp.einsum(
-        "nthd,hdv->nthv", query_start, entering, precision=HIGHEST
-    )
-    attention_output = attention_output.reshape(tokens, local_head_count, DV)
-    inverse_rms = lax.rsqrt(
-        jnp.mean(attention_output * attention_output, axis=-1, keepdims=True) + EPSILON
-    )
-    gate_act = jax.nn.silu(
-        output_gate_preactivation.astype(jnp.float32).reshape(tokens, local_head_count, DV)
-    )
-    head_rows = (
-        (attention_output * inverse_rms * head_norm_gain.astype(jnp.float32) * gate_act)
-        .reshape(tokens, local_head_count * DV)
-        .astype(jnp.bfloat16)
-    )
-    tp_steps = [("tp", bit) for bit in range(lax.axis_size("tp").bit_length() - 1)][::-1]
-    projected = jnp.dot(
-        spread(head_rows, tp_steps),
-        relative_rows(output_projection, lax.axis_index("tp"), masks_of(tp_steps, "tp")),
-        preferred_element_type=jnp.float32,
-    )
-    mid_local = (residual.astype(jnp.float32) + projected).astype(jnp.bfloat16)
-    most = 3 * tokens * routing.shape[1] // (2 * lax.axis_size("sp"))
     if lax.axis_size("tp") == FF_PARTS and lax.axis_size("sp") == 8:
+        mid_local = attend_project(
+            queries,
+            key_matrix,
+            value_matrix,
+            output_gate_preactivation,
+            decay_preactivation,
+            extra_log_decay,
+            head_norm_gain,
+            residual,
+            output_projection,
+        )
         return exchange_experts(
             mid_local,
             feedforward_gain,
@@ -937,6 +1180,37 @@
             shared_expert_up,
             shared_expert_down,
         )
+    local_part, query_start, dev_decay, dev_update = attention_heads(
+        queries, key_matrix, value_matrix, decay_preactivation, extra_log_decay
+    )
+    _, entering = prefix(
+        (dev_decay, dev_update),
+        "sp",
+        carry_combine,
+        (jnp.ones_like(dev_decay), jnp.zeros_like(dev_update)),
+    )
+    attention_output = local_part + jnp.einsum(
+        "nthd,hdv->nthv", query_start, entering, precision=HIGHEST
+    )
+    attention_output = attention_output.reshape(tokens, local_head_count, DV)
+    inverse_rms = lax.rsqrt(
+        jnp.mean(attention_output * attention_output, axis=-1, keepdims=True) + EPSILON
+    )
+    gate_act = jax.nn.silu(
+        output_gate_preactivation.astype(jnp.float32).reshape(tokens, local_head_count, DV)
+    )
+    head_rows = (
+        (attention_output * inverse_rms * head_norm_gain.astype(jnp.float32) * gate_act)
+        .reshape(tokens, local_head_count * DV)
+        .astype(jnp.bfloat16)
+    )
+    tp_steps = [("tp", bit) for bit in range(lax.axis_size("tp").bit_length() - 1)][::-1]
+    projected = jnp.dot(
+        spread(head_rows, tp_steps),
+        relative_rows(output_projection, lax.axis_index("tp"), masks_of(tp_steps, "tp")),
+        preferred_element_type=jnp.float32,
+    )
+    mid_local = (residual.astype(jnp.float32) + projected).astype(jnp.bfloat16)
     mid_rows = lax.all_gather(mid_local, "tp", axis=1, tiled=True).astype(jnp.float32)
     normed = (
         mid_rows

time: 184 us -> 141 us (0.77)
  Pallas kernels: 116 us -> 136 us
  waiting for transfers between devices: 19.1 us -> 0 us
  matrix products: 16.7 us -> 0 us
  starting transfers between devices: 12.9 us -> 0 us
  local copies, waits for them, and re-layouts: 11.8 us -> 4.19 us
  other arithmetic: 6.42 us -> 0 us
    pallas_call x0 -> x1, Pallas kernels: none -> 24.1 us  [attend_project(): pl.pallas_call(attend_kernel, name='attend_project', out_shape=jax.ShapeD...]
    ppermute x7 -> x0, waiting for transfers between devices: 19.1 us -> none  [from_partner(): return lax.ppermute(value, axis, pairs)]
    dot_general x7 -> x0, matrix products: 16.7 us -> none  [the longest x1 6.09 us: attention_heads(): jnp.einsum('nmhd,mhdv->nhdv', jnp.exp(span_logs), update, precision=HIGHEST)]
    ppermute x7 -> x0, starting transfers between devices: 12.9 us -> none  [from_partner(): return lax.ppermute(value, axis, pairs)]
    pallas_call x1, Pallas kernels: 116 us -> 112 us  [exchange_experts(): pl.pallas_call(functools.partial(exchange_kernel, most), name='exchange_e...]
    convert_element_type x8 -> x0, other arithmetic: 2.62 us -> none  [the longest x4 2.21 us: prefix(): a.astype(jnp.bfloat16)]
    dynamic_slice x1 -> x0, local copies, waits for them, and re-layouts: 2.49 us -> none  [relative_rows(): lax.dynamic_slice_in_dim(matrix, (place ^ mask) * height, height, 0)]
    add x3 -> x0, local copies, waits for them, and re-layouts: 2.41 us -> none  [the longest x1 0.87 us: attention_heads(): log_decay_rows + extra_log_decay.reshape(block_count, BLOCK_POSITIONS, lo...]
  transfers between devices with their start and end apart: 7 -> 0, of which waited for: 4 -> 0; matrix products, arithmetic and copies ran while one was open for 12% -> 0% of each run, Pallas kernels for 0% -> 0%
where the time goes in v2:
time: 141 us; the launch traced here: 140 us
  Pallas kernels  136 us (96%)
  local copies, waits for them, and re-layouts  4.19 us (3%)
    pallas_call x1, Pallas kernels, exchange_experts(): pl.pallas_call(functools.partial(exchange_kernel, most), name='exchange_e...  112 us
    pallas_call x1, Pallas kernels, attend_project(): pl.pallas_call(attend_kernel, name='attend_project', out_shape=jax.ShapeD...  24.1 us

profile of v2, /device:TPU:0, one launch (start us, length us, event | category | flops | bytes accessed | tf_op | source)
XLA Modules:
  0.0 140.5 jit_solution(6417733696126660002)
XLA Ops:
  0.0 1.2 reshape.6.norm_gain_ref
  1.2 1.3 reshape.7.gain_ref
  2.5 24.1 %attend_project.1.mid_ref = bf16[256,512]{1,0:T(8,128)(2,1)} custom-call(f32[4,256]{1,0:T(4,128)} %bitcast.3, bf16[1,256]{1,0:T(2,128)(2,1)} %reshape.6.norm_gain_ref, bf16[256,512]{1,0:T(8,128)(2,1)} %decay_hbm.1, bf16[256,512]{1,0:T(8,128)(2,1)} %key_hbm.1, bf16[256,1024]{1,0:T(8,128)(2,1)} %value_hbm.1, bf16[256,512]{1,0:T(8,128)(2,1)} %query_hbm.1, ...), custom_call_target="tpu_custom_call" | custom-call | tf_op jit(solution)/shard_map/attend_project/pallas_call | solution.py:1052
  26.7 112.1 %exchange_experts.1 = bf16[256,512]{1,0:T(8,128)(2,1)} custom-call(bf16[256,512]{1,0:T(8,128)(2,1)} %attend_project.1.mid_ref, bf16[1,2048]{1,0:T(2,128)(2,1)} %reshape.7.gain_ref, s32[4,256]{1,0:T(4,128)} %bitcast.4, f32[4,256]{1,0:T(4,128)} %bitcast.5, bf16[2048,256]{1,0:T(8,128)(2,1)} %gate_hbm.3, bf16[2048,256]{1,0:T(8,128)(2,1)} %up_hbm.1, ...), custom_call_target="tpu_custom_call" | custom-call | tf_op jit(solution)/shard_map/exchange_experts/pallas_call | solution.py:673
  138.8 1.7 %copy.20 = bf16[256,512]{1,0:T(8,128)(2,1)} copy(bf16[256,512]{1,0:T(8,128)(2,1)} %exchange_experts.1) | data formatting | bytes 524288

commit v3 on v2

--- a/solution.py
+++ b/solution.py
@@ -137,6 +137,7 @@
     ranks,
     slot_weights,
     picks,
+    turned,
     own_rows,
     partner_high,
     core_rows,
@@ -307,10 +308,18 @@
 
     def pick_block(depth_at):
         source = depth_at * 2 + x
-        for number, expert in ((0, sp), (1, z * 2 + 1 - x)):
-            picks[depth_at, pl.ds(number * most, most), :] = (
-                jnp.where(pick(source, expert), 1.0, 0.0).astype(bf16)
-            )
+        chosen = jnp.concatenate(
+            [
+                jnp.where(pick(source, expert), 1.0, 0.0)
+                for expert in (sp, z * 2 + 1 - x)
+            ],
+            axis=0,
+        )
+        picks[depth_at] = chosen.astype(bf16)
+
+    def turn():
+        for depth_at in range(depth):
+            turned[depth_at] = picks[depth_at].astype(f32).T.astype(bf16)
 
     def prepare(depth_at, first):
         for source in (depth_at * 2 + x, depth_at * 2 + 1 - x):
@@ -344,46 +353,60 @@
         ref = expert_rows.at[held[0], source]
         begin(remote(ref, ref, y_send.at[source], y_recv.at[source], over_y))
 
-    def lines(k):
-        at = order[k]
+    def compact(at, part, number, rows):
         source = at * 2 + x
+        chosen = jnp.dot(picks[at], rows, preferred_element_type=f32).astype(bf16)
+        side_out[at, part] = chosen[most:]
+        begin(
+            remote(
+                side_out.at[at, part],
+                expert_rows.at[number, source],
+                side_send.at[at, part],
+                side_recv.at[at, part],
+                side,
+            )
+        )
+        expert_rows[number, source] = chosen[:most]
+
+    def own_block():
+        source = sp
         for part in range(EXPERT_PARTS):
-            if k > 0:
-                ref = line_rows.at[at, part]
-                arrive(ref, line_recv.at[at, part])
-                begin(
-                    remote(ref, ref, left_send.at[at, part], line_recv.at[at, part], left),
-                    jnp.logical_and(at > z, has_left),
-                )
-                begin(
-                    remote(ref, ref, right_send.at[at, part], line_recv.at[at, part], right),
-                    jnp.logical_and(at < z, has_right),
-                )
-                rows = line_rows[at, part]
-            else:
-                rows = line_rows[z, 2] if part == 2 else own_rows[part]
-            chosen = jnp.dot(picks[at], rows, preferred_element_type=f32).astype(bf16)
-            side_out[at, part] = chosen[most:]
-            begin(
-                remote(
-                    side_out.at[at, part],
-                    expert_rows.at[held[part], source],
-                    side_send.at[at, part],
-                    side_recv.at[at, part],
-                    side,
-                )
-            )
-            expert_rows[held[part], source] = chosen[:most]
-            if part == 0 and k > 0:
-                to_y(source)
+            rows = line_rows[z, 2] if part == 2 else own_rows[part]
+            compact(z, part, held[part], rows)
             to_core(held[part], source)
-        if k == 0:
-            arrive(partner_high, own_recv.at[1])
-            begin(remote(partner_high, core_rows.at[3], core_send.at[3], core_recv.at[3], over_core))
-            expert_rows[late, source] = jnp.dot(
-                picks[at, pl.ds(0, most), :], partner_high[...], preferred_element_type=f32
-            ).astype(bf16)
-            to_core(late, source)
+        arrive(partner_high, own_recv.at[1])
+        begin(remote(partner_high, core_rows.at[3], core_send.at[3], core_recv.at[3], over_core))
+        expert_rows[late, source] = jnp.dot(
+            picks[z, pl.ds(0, most), :], partner_high[...], preferred_element_type=f32
+        ).astype(bf16)
+        to_core(late, source)
+
+    inner = jnp.logical_and(has_left, has_right)
+    turns = [(1, 0), (2, 0), (1, 1), (2, 1), (1, 2), (2, 2), (3, 0), (3, 1), (3, 2)]
+
+    def line(number):
+        (k, part), (plain_k, plain_part) = turns[number], divmod(number, EXPERT_PARTS)
+        at = jnp.where(inner, order[k], order[plain_k + 1])
+        part = jnp.where(inner, part, plain_part)
+        ref = line_rows.at[at, part]
+        arrive(ref, line_recv.at[at, part])
+        begin(
+            remote(ref, ref, left_send.at[at, part], line_recv.at[at, part], left),
+            jnp.logical_and(at > z, has_left),
+        )
+        begin(
+            remote(ref, ref, right_send.at[at, part], line_recv.at[at, part], right),
+            jnp.logical_and(at < z, has_right),
+        )
+        part_number = jnp.where(part == 0, held[0], jnp.where(part == 1, held[1], held[2]))
+        compact(at, part, part_number, line_rows[at, part])
+        source = at * 2 + x
+        ref = expert_rows.at[part_number, source]
+        begin(
+            remote(ref, ref, y_send.at[source], y_recv.at[source], over_y),
+            part == 0,
+        )
+        to_core(part_number, source)
 
     def sides(k):
         at = order[k]
@@ -491,9 +514,7 @@
     def spread_back(at, part):
         arrive(side_in.at[at, part], back_side_recv.at[at, part])
         rows = jnp.concatenate([results[at * 2 + x, part], side_in[at, part]], axis=0)
-        return lax.dot_general(
-            picks[at], rows, (((0,), (0,)), ((), ())), preferred_element_type=f32
-        )
+        return jnp.dot(turned[at], rows, preferred_element_type=f32)
 
     def arrived(at, part):
         from_right = jnp.logical_and(at <= z, has_right)
@@ -585,35 +606,43 @@
             joined, shared_down_ref[...], preferred_element_type=f32
         )
 
-    lines(0)
-    for k in range(1, depth):
-        prepare(order[k], False)
+    own_block()
+    prepare(order[1], False)
+    line(0)
+    prepare(order[2], False)
+    line(1)
+    line(2)
+    line(3)
+    sides(0)
+    prepare(order[3], False)
+    line(4)
+    lates(0, 1)
     for load in loads:
         load.wait()
-    sides(0)
+    line(5)
+    experts(0)
+    line(6)
+    sides(1)
+    line(7)
+    pairs(0)
+    line(8)
     shared_first()
-    lines(1)
-    lates(0, 1)
-    experts(0)
-    sides(1)
-    lines(2)
+    sides(2)
     lates(1, 0)
     lates(1, 1)
     experts(1)
-    pairs(0)
-    sides(2)
-    lines(3)
+    ready(0)
+    pairs(1)
+    turn()
     lates(2, 0)
     lates(2, 1)
     experts(2)
-    pairs(1)
-    ready(0)
     sides(3)
+    ready(1)
+    pairs(2)
     lates(3, 0)
     lates(3, 1)
     experts(3)
-    pairs(2)
-    ready(1)
     pairs(3)
     ready(2)
     back_lines(0)
@@ -683,6 +712,7 @@
             vmem((sp_count, sp_count, tokens), f32),
             vmem((sp_count, most, 128), f32),
             vmem((depth, 2 * most, tokens), bf16),
+            vmem((depth, tokens, 2 * most), bf16),
             vmem((2, tokens, half), bf16),
             vmem((tokens, half), bf16),
             vmem((4, tokens, half), bf16),

time: 141 us -> 133 us (0.943)
  Pallas kernels: 136 us -> 128 us
    pallas_call x1, Pallas kernels: 112 us -> 104 us  [exchange_experts(): pl.pallas_call(functools.partial(exchange_kernel, most), name='exchange_e...]
where the time goes in v3:
time: 133 us; the launch traced here: 132 us
  Pallas kernels  128 us (96%)
  local copies, waits for them, and re-layouts  4.19 us (3%)
    pallas_call x1, Pallas kernels, exchange_experts(): pl.pallas_call(functools.partial(exchange_kernel, most), name='exchange_e...  104 us
    pallas_call x1, Pallas kernels, attend_project(): pl.pallas_call(attend_kernel, name='attend_project', out_shape=jax.ShapeD...  24.1 us

profile of v3, /device:TPU:0, one launch (start us, length us, event | category | flops | bytes accessed | tf_op | source)
XLA Modules:
  0.0 132.4 jit_solution(9941552461144322329)
XLA Ops:
  0.0 1.2 reshape.6.norm_gain_ref
  1.2 1.3 reshape.7.gain_ref
  2.5 24.1 %attend_project.1.mid_ref = bf16[256,512]{1,0:T(8,128)(2,1)} custom-call(f32[4,256]{1,0:T(4,128)} %bitcast.3, bf16[1,256]{1,0:T(2,128)(2,1)} %reshape.6.norm_gain_ref, bf16[256,512]{1,0:T(8,128)(2,1)} %decay_hbm.1, bf16[256,512]{1,0:T(8,128)(2,1)} %key_hbm.1, bf16[256,1024]{1,0:T(8,128)(2,1)} %value_hbm.1, bf16[256,512]{1,0:T(8,128)(2,1)} %query_hbm.1, ...), custom_call_target="tpu_custom_call" | custom-call | tf_op jit(solution)/shard_map/attend_project/pallas_call | solution.py:1082
  26.7 104.1 %exchange_experts.1 = bf16[256,512]{1,0:T(8,128)(2,1)} custom-call(bf16[256,512]{1,0:T(8,128)(2,1)} %attend_project.1.mid_ref, bf16[1,2048]{1,0:T(2,128)(2,1)} %reshape.7.gain_ref, s32[4,256]{1,0:T(4,128)} %bitcast.4, f32[4,256]{1,0:T(4,128)} %bitcast.5, bf16[2048,256]{1,0:T(8,128)(2,1)} %gate_hbm.3, bf16[2048,256]{1,0:T(8,128)(2,1)} %up_hbm.1, ...), custom_call_target="tpu_custom_call" | custom-call | tf_op jit(solution)/shard_map/exchange_experts/pallas_call | solution.py:702
  130.8 1.7 %copy.20 = bf16[256,512]{1,0:T(8,128)(2,1)} copy(bf16[256,512]{1,0:T(8,128)(2,1)} %exchange_experts.1) | data formatting | bytes 524288

commit v4 on v3

--- a/solution.py
+++ b/solution.py
@@ -638,8 +638,8 @@
     lates(2, 1)
     experts(2)
     sides(3)
+    pairs(2)
     ready(1)
-    pairs(2)
     lates(3, 0)
     lates(3, 1)
     experts(3)
@@ -795,6 +795,7 @@
     decays_in,
     state_out,
     state_in,
+    carry_first,
     carry_out,
     carry_in,
     local_mixed,
@@ -965,33 +966,43 @@
         local_mixed[head] = jnp.concatenate(pieces, axis=0)
         query_start[head] = jnp.concatenate(starts, axis=0).astype(bf16)
 
-    def chain(head):
+    def joined(head):
         wide = columns(head, DK)
-        arrive(state_in.at[head], state_recv.at[head])
         own, other = state_out[head].astype(f32), state_in[head].astype(f32)
-        decay_own, decay_other = decays[0:1, wide], decays_in[0:1, wide]
         first = jnp.where(x == 0, own, other)
         second = jnp.where(x == 0, other, own)
-        decay_second = jnp.where(x == 0, decay_other, decay_own)
-
-        @pl.when(has_left)
-        def _():
-            arrive(carry_in.at[head], carry_recv.at[head])
-
-        entering = jnp.where(has_left, carry_in[head].astype(f32), 0.0)
-        carry_out[head] = (
-            decay_own * decay_other * entering + decay_second * first + second
-        ).astype(bf16)
+        decay_second = jnp.where(x == 0, decays_in[0:1, wide], decays[0:1, wide])
+        return decay_second * first + second
+
+    def give(source, head, when):
         begin(
             remote(
-                carry_out.at[head],
+                source.at[head],
                 carry_in.at[head],
                 carry_send.at[head],
                 carry_recv.at[head],
                 right,
             ),
-            has_right,
-        )
+            when,
+        )
+
+    def lead(head):
+        arrive(state_in.at[head], state_recv.at[head])
+        carry_first[head] = joined(head).astype(bf16)
+        give(carry_first, head, jnp.logical_not(has_left))
+
+    def chain(head):
+        wide = columns(head, DK)
+        decay_own, decay_other = decays[0:1, wide], decays_in[0:1, wide]
+
+        @pl.when(has_left)
+        def _():
+            arrive(carry_in.at[head], carry_recv.at[head])
+
+        entering = jnp.where(has_left, carry_in[head].astype(f32), 0.0)
+        carry_out[head] = (decay_own * decay_other * entering + joined(head)).astype(bf16)
+        give(carry_out, head, jnp.logical_and(has_left, has_right))
+        other = state_in[head].astype(f32)
         return jnp.where(x == 0, entering, decay_other * entering + other).astype(bf16)
 
     def finish(head, entering):
@@ -1021,10 +1032,13 @@
         begin(remote(target, target, pass_send.at[head], pass_recv.at[head], over_core))
 
     loads[3].wait()
+    local(0)
+    arrive(decays_in, decay_sems.at[2])
     for head in range(head_count):
-        local(head)
+        lead(head)
+        if head + 1 < head_count:
+            local(head + 1)
     loads[4].wait()
-    arrive(decays_in, decay_sems.at[2])
     for head in range(head_count):
         entering = chain(head)
         finish(head, entering)
@@ -1091,6 +1105,7 @@
             vmem((head_count, tokens, DK), bf16),
             vmem((8, head_count * DK), f32),
             vmem((8, head_count * DK), f32),
+            vmem((head_count, DV, DK), bf16),
             vmem((head_count, DV, DK), bf16),
             vmem((head_count, DV, DK), bf16),
             vmem((head_count, DV, DK), bf16),

time: 133 us -> 133 us (level)
    pallas_call x1, Pallas kernels: 24.1 us -> 28.4 us  [attend_project(): pl.pallas_call(attend_kernel, name='attend_project', out_shape=jax.ShapeD...]
    pallas_call x1, Pallas kernels: 104 us -> 100 us  [exchange_experts(): pl.pallas_call(functools.partial(exchange_kernel, most), name='exchange_e...]
where the time goes in v4:
time: 133 us
  Pallas kernels  129 us (97%)
  local copies, waits for them, and re-layouts  4.19 us (3%)
    pallas_call x1, Pallas kernels, exchange_experts(): pl.pallas_call(functools.partial(exchange_kernel, most), name='exchange_e...  100 us
    pallas_call x1, Pallas kernels, attend_project(): pl.pallas_call(attend_kernel, name='attend_project', out_shape=jax.ShapeD...  28.4 us

profile of v4, /device:TPU:0, one launch (start us, length us, event | category | flops | bytes accessed | tf_op | source)
XLA Modules:
  0.0 133.0 jit_solution(2884878526588374691)
XLA Ops:
  0.0 1.2 reshape.6.norm_gain_ref
  1.2 1.3 reshape.7.gain_ref
  2.5 28.4 %attend_project.1.mid_ref = bf16[256,512]{1,0:T(8,128)(2,1)} custom-call(f32[4,256]{1,0:T(4,128)} %bitcast.3, bf16[1,256]{1,0:T(2,128)(2,1)} %reshape.6.norm_gain_ref, bf16[256,512]{1,0:T(8,128)(2,1)} %decay_hbm.1, bf16[256,512]{1,0:T(8,128)(2,1)} %key_hbm.1, bf16[256,1024]{1,0:T(8,128)(2,1)} %value_hbm.1, bf16[256,512]{1,0:T(8,128)(2,1)} %query_hbm.1, ...), custom_call_target="tpu_custom_call" | custom-call | tf_op jit(solution)/shard_map/attend_project/pallas_call | solution.py:1096
  30.9 100.4 %exchange_experts.1 = bf16[256,512]{1,0:T(8,128)(2,1)} custom-call(bf16[256,512]{1,0:T(8,128)(2,1)} %attend_project.1.mid_ref, bf16[1,2048]{1,0:T(2,128)(2,1)} %reshape.7.gain_ref, s32[4,256]{1,0:T(4,128)} %bitcast.4, f32[4,256]{1,0:T(4,128)} %bitcast.5, bf16[2048,256]{1,0:T(8,128)(2,1)} %gate_hbm.3, bf16[2048,256]{1,0:T(8,128)(2,1)} %up_hbm.1, ...), custom_call_target="tpu_custom_call" | custom-call | tf_op jit(solution)/shard_map/exchange_experts/pallas_call | solution.py:702
  131.4 1.7 %copy.20 = bf16[256,512]{1,0:T(8,128)(2,1)} copy(bf16[256,512]{1,0:T(8,128)(2,1)} %exchange_experts.1) | data formatting | bytes 524288
